TPU v7x, 512 devices: a 4x2x32 block of a 4x8x32 slice. The times are simulated.
512 devices in a mesh: grp: 2 (over y), fs: 32 (over z), tp: 8 (over x, core).
Axes of the slice: x: 4, y: 2, z: 32, core: 2. Of those that a mesh axis runs over, the one named last changes fastest.
The devices are a block of a 4x8x32 slice.
Arguments:
- tokens: bfloat16 [64, 384, 2048], P(('grp', 'fs'), None, 'tp'), parts along dimension 0, may hold values from -16 to 16
- norm_gain: float32 [2048], P('tp'), may hold values from 0.1 to 1.9
- in_weight: bfloat16 [2048, 1024], P('fs', 'tp'), may hold values from -0.125 to 0.125
- pool_weight: bfloat16 [8, 128, 128], P('tp'), may hold values from -0.5 to 0.5
- pool_scale: float32 [1024], P('tp'), may hold values from 0.1 to 1.9
- out_weight: bfloat16 [1024, 2048], P('fs', 'tp'), may hold values from -0.1875 to 0.1875
- ffn_gain: float32 [2048], P('tp'), may hold values from 0.1 to 1.9
- gate_weight: bfloat16 [2048, 5632], P('fs', 'tp'), may hold values from -0.125 to 0.125
- up_weight: bfloat16 [2048, 5632], P('fs', 'tp'), may hold values from -0.125 to 0.125
- down_weight: bfloat16 [5632, 2048], P('tp', 'fs'), may hold values from -0.078125 to 0.078125
Outputs:
- output: bfloat16 [64, 384, 2048], P(('grp', 'fs'), None, 'tp'), parts along dimension 0
There are 2 independent parts, one for each index of `grp`. A program takes and returns all parts, laid end to end along the dimension named above; an argument that names none is the same for every part. Nothing has to cross between parts.
All inputs are finite; a program needn't handle non-finite values.
Results may differ from a plain program's by a relative error of at most 0.009.
Values may be sent and summed in bfloat16 or wider, within the bound.
No kernel may reach another device: no remote copies, remote signals or barrier semaphores. Data moves between devices by JAX's collectives and lax.ppermute only.
A program may use at most 64 MiB of HBM per device.

v0:
```python
import jax
import jax.numpy as jnp
from jax import lax
from jax.sharding import PartitionSpec as P

D = 2048
GD = 128


EPSILON = 0.05
HALVES = (1, 2, 4, 8)


def sent_to_all(array, axis):
    copies = jnp.broadcast_to(array, (lax.axis_size(axis), *array.shape))
    return lax.all_to_all(copies, axis, split_axis=0, concat_axis=0, tiled=True)


def over_copies(array, axis):
    everything = sent_to_all(array, axis)
    return jnp.sum(everything, axis=0)


def laid_out(tiles, dim):
    tiles = jnp.moveaxis(tiles, 0, dim)
    shape = tiles.shape
    return tiles.reshape(*shape[:dim], shape[dim] * shape[dim + 1], *shape[dim + 2 :])


def collect(array, axis, dim):
    return laid_out(sent_to_all(array, axis), dim)


def gather_turned(arrays, axis, dims):
    turned = [jnp.moveaxis(a, dim, 0) for a, dim in zip(arrays, dims)]
    both = jnp.concatenate([t.reshape(len(t), -1) for t in turned], axis=1)
    out, at, outs = (lax.all_gather(both, axis, axis=0, tiled=True), 0, [])
    for t, dim in zip(turned, dims):
        piece = out[:, at : at + t[0].size].reshape(-1, *t.shape[1:])
        outs.append(jnp.moveaxis(piece, 0, dim))
        at += t[0].size
    return tuple(outs)


def split_up(array, dim, length):
    before, after = (array.shape[:dim], array.shape[dim + 1 :])
    return jnp.moveaxis(array.reshape(*before, length, -1, *after), dim, 0)


def sum_at_owner(array, axis, dim):
    tiles = split_up(array, dim, lax.axis_size(axis))
    arrived = lax.all_to_all(tiles, axis, split_axis=0, concat_axis=0, tiled=True)
    return arrived.astype(jnp.float32).sum(axis=0)


def local(
    tokens,
    norm_gain,
    in_weight,
    pool_weight,
    pool_scale,
    out_weight,
    ffn_gain,
    gate_weight,
    up_weight,
    down_weight,
):
    seq_local, length, feat_local = tokens.shape
    stream = tokens.astype(jnp.float32)
    first_square = over_copies(jnp.sum(stream * stream, axis=-1), "tp")
    normed = (stream * lax.rsqrt(first_square[..., None] / D + EPSILON) * norm_gain).astype(
        jnp.bfloat16
    )
    in_full = collect(in_weight, "fs", 0)
    channels = in_full.shape[1]
    weight_rows = in_full
    pool_input = jnp.einsum(
        "slk,kc->slc", collect(normed, "tp", 2), weight_rows, preferred_element_type=jnp.float32
    ).astype(jnp.bfloat16)
    pool_float = pool_input.astype(jnp.float32)
    group_local = pool_weight.shape[0]
    group_ids = lax.axis_index("tp") * group_local + jnp.arange(channels) // GD
    selector = group_ids % 4
    running = jnp.concatenate(
        [jnp.zeros((seq_local, 1, channels), jnp.float32), jnp.cumsum(pool_float, axis=1)], axis=1
    )
    position = jnp.arange(length)
    window_mean = jnp.zeros_like(pool_float)
    for window_index, half_width in enumerate(HALVES):
        upper_sum = jnp.concatenate(
            [running[:, half_width:], jnp.repeat(running[:, -1:], half_width, axis=1)], axis=1
        )[:, :length]
        lower_sum = jnp.concatenate(
            [
                jnp.zeros((seq_local, half_width, channels), jnp.float32),
                running[:, : length + 1 - half_width],
            ],
            axis=1,
        )[:, :length]
        counts = (
            jnp.minimum(position + half_width, length) - jnp.maximum(position - half_width, 0)
        ).astype(jnp.float32)
        window_mean = jnp.where(
            selector == window_index, (upper_sum - lower_sum) / counts[:, None], window_mean
        )
    deviation = (window_mean - pool_float).astype(jnp.bfloat16)
    grouped = deviation.reshape(seq_local, length, group_local, GD)
    mapped = jnp.einsum("slgc,gcd->slgd", grouped, pool_weight, preferred_element_type=jnp.float32)
    pooled = (mapped.reshape(seq_local, length, channels) * pool_scale).astype(jnp.bfloat16)
    out_full = collect(out_weight, "fs", 0)
    weight_rows = out_full
    mixed = stream + jnp.einsum(
        "jut,tx->jux", collect(pooled, "tp", 2), weight_rows, preferred_element_type=jnp.float32
    )
    second_square = over_copies(jnp.sum(mixed * mixed, axis=-1), "tp")
    normed_two = (mixed * lax.rsqrt(second_square[..., None] / D + EPSILON) * ffn_gain).astype(
        jnp.bfloat16
    )
    features_full = collect(normed_two, "tp", 2)
    gate_full, up_full, down_full = gather_turned(
        (gate_weight, up_weight, down_weight), "fs", (0, 0, 1)
    )
    gate_out = jnp.einsum(
        "slk,kf->slf", features_full, gate_full, preferred_element_type=jnp.float32
    )
    up_out = jnp.einsum("slk,kf->slf", features_full, up_full, preferred_element_type=jnp.float32)
    hidden = (jax.nn.silu(gate_out) * up_out).astype(jnp.bfloat16)
    partial_value = jnp.einsum("hor,rn->hon", hidden, down_full, preferred_element_type=jnp.float32)
    summed = sum_at_owner(partial_value.astype(jnp.bfloat16), "tp", 2)
    return (mixed + summed).astype(jnp.bfloat16)


def solution(mesh):
    return jax.shard_map(
        local,
        mesh=mesh,
        in_specs=(
            P(("grp", "fs"), None, "tp"),
            P("tp"),
            P("fs", "tp"),
            P("tp", None, None),
            P("tp"),
            P("fs", "tp"),
            P("tp"),
            P("fs", "tp"),
            P("fs", "tp"),
            P("tp", "fs"),
        ),
        out_specs=P(("grp", "fs"), None, "tp"),
        check_vma=False,
    )
```

profile of v0, /device:TPU:33, one launch (start us, length us, event | category | flops | bytes accessed | tf_op | source)
XLA Modules:
  0.0 331.7 jit_solution(415555806456756813)
XLA Ops:
  6.6 1.8 concatenate.35
  8.5 1.1 copy.44
  9.6 48.5 %all_to_all.40 = f32[8,1,384]{2,1,0:T(1,128)S(1)} all-to-all(f32[8,1,384]{2,1,0:T(1,128)S(1)} %broadcast_in_dim.49), channel_id=1, replica_groups=mesh['grp'=2,'fs'=32,'tp'=8] {'tp'}, dimensions={0} | all-to-all | bytes 24576 | tf_op jit(solution)/shard_map/all_to_all | solution.py:16
  58.2 0.8 fusion.45
  59.1 23.8 %all_to_all.41 = bf16[8,1,384,256]{2,3,1,0:T(8,128)(2,1)S(1)} all-to-all(bf16[8,1,384,256]{2,3,1,0:T(8,128)(2,1)S(1)} %broadcast_in_dim.50), channel_id=1, replica_groups=mesh['grp'=2,'fs'=32,'tp'=8] {'tp'}, dimensions={0} | all-to-all | bytes 3145728 | tf_op jit(solution)/shard_map/all_to_all | solution.py:16
  83.0 75.0 %all_to_all.42 = bf16[32,64,128]{2,1,0:T(8,128)(2,1)S(1)} all-to-all(bf16[32,64,128]{2,1,0:T(8,128)(2,1)S(1)} %broadcast_in_dim.51), channel_id=1, replica_groups=mesh['grp'=2,'fs'=32,'tp'=8] {'fs'}, dimensions={0} | all-to-all | bytes 1048576 | tf_op jit(solution)/shard_map/all_to_all | solution.py:16
  158.0 0.9 broadcast_in_dim.57
  159.0 5.3 %all-to-all-start.4 = ((bf16[32,32,256]{2,1,0:T(8,128)(2,1)}), bf16[32,32,256]{2,1,0:T(8,128)(2,1)S(1)}, u32[]{:S(2)}, u32[]{:S(2)}) async-start(bf16[32,32,256]{2,1,0:T(8,128)(2,1)} %broadcast_in_dim.57), calls=%async_computation.4 | async-start | bytes 1048576 | tf_op jit(solution)/shard_map/all_to_all | solution.py:16
  164.4 0.6 fusion.18
  165.4 0.4 copy-done.4
  165.9 0.4 fusion.16
  166.4 65.4 %all-to-all-done.4 = bf16[32,32,256]{2,1,0:T(8,128)(2,1)S(1)} async-done(((bf16[32,32,256]{2,1,0:T(8,128)(2,1)}), bf16[32,32,256]{2,1,0:T(8,128)(2,1)S(1)}, u32[]{:S(2)}, u32[]{:S(2)}) %all-to-all-start.4) | async-done | bytes 524320 | tf_op jit(solution)/shard_map/all_to_all | solution.py:16
  231.9 19.3 %all_to_all.43 = bf16[8,1,384,128]{2,3,1,0:T(8,128)(2,1)S(1)} all-to-all(bf16[8,1,384,128]{2,3,1,0:T(8,128)(2,1)S(1)} %broadcast_in_dim.56), channel_id=1, replica_groups=mesh['grp'=2,'fs'=32,'tp'=8] {'tp'}, dimensions={0} | all-to-all | bytes 1572864 | tf_op jit(solution)/shard_map/all_to_all | solution.py:16
  251.3 0.5 multiply_reduce_fusion
  251.8 8.0 %all_to_all.44 = f32[8,1,384]{2,1,0:T(1,128)S(1)} all-to-all(f32[8,1,384]{2,1,0:T(1,128)S(1)} %broadcast_in_dim.58), channel_id=1, replica_groups=mesh['grp'=2,'fs'=32,'tp'=8] {'tp'}, dimensions={0} | all-to-all | bytes 24576 | tf_op jit(solution)/shard_map/all_to_all | solution.py:16
  260.2 23.8 %all_to_all.45 = bf16[8,1,384,256]{2,3,1,0:T(8,128)(2,1)S(1)} all-to-all(bf16[8,1,384,256]{2,3,1,0:T(8,128)(2,1)S(1)} %broadcast_in_dim.59), channel_id=1, replica_groups=mesh['grp'=2,'fs'=32,'tp'=8] {'tp'}, dimensions={0} | all-to-all | bytes 3145728 | tf_op jit(solution)/shard_map/all_to_all | solution.py:16
  283.9 4.6 %fusion.4 = f32[384,704]{0,1:T(8,128)} fusion(bf16[384,2048]{0,1:T(8,128)(2,1)S(1)} %bitcast.89, bf16[2048,2112]{1,0:T(8,128)(2,1)} %all-gather.2.cloned.1.call-done), kind=kOutput, calls=%fused_computation.4 | convolution fusion | flops 1107296256 | bytes 5799936 | tf_op jit(solution)/shard_map/slk,kf->slf/dot_general | solution.py:123
  288.5 8.8 %fusion.6 = bf16[384,2048]{1,0:T(8,128)(2,1)} fusion(bf16[2048,2112]{1,0:T(8,128)(2,1)} %all-gather.2.cloned.1.call-done, bf16[384,2048]{0,1:T(8,128)(2,1)S(1)} %bitcast.90, f32[384,704]{0,1:T(8,128)} %fusion.4), kind=kOutput, calls=%fused_computation.7 | convolution fusion | flops 2217000960 | bytes 10518528 | tf_op jit(solution)/shard_map/hor,rn->hon/dot_general | solution.py:128
  297.3 1.9 copy.60
  299.2 0.3 copy.64
  299.5 24.1 %all_to_all.46 = bf16[8,1,384,256]{3,2,1,0:T(8,128)(2,1)S(1)} all-to-all(bf16[8,1,384,256]{3,2,1,0:T(8,128)(2,1)S(1)} %bitcast.85), channel_id=1, replica_groups=mesh['grp'=2,'fs'=32,'tp'=8] {'tp'}, dimensions={0} | all-to-all | bytes 3145728 | tf_op jit(solution)/shard_map/all_to_all | solution.py:52
  323.6 0.2 convert_reduce_fusion
  323.8 0.2 copy.55
  324.1 0.8 copy.56
  (44 shorter events, 1.3 us)
Async XLA Ops:
  6.5 158.9 %copy-start = (bf16[1,128,128]{2,1,0:T(8,128)(2,1)S(1)}, bf16[1,128,128]{2,1,0:T(8,128)(2,1)}, u32[]{:S(2)}) copy-start(bf16[1,128,128]{2,1,0:T(8,128)(2,1)} %param.13) | copy-start | bytes 98308
  6.6 277.4 %all-gather.2.cloned.1.call-start = ((), (), s32[]{:S(2)}) async-start(), calls=%async_computation.8 | async-start | bytes 9191424 | tf_op jit(solution)/shard_map/all_gather | solution.py:37
  59.1 23.8 %copy-start.1 = (bf16[64,128]{1,0:T(8,128)(2,1)S(1)}, bf16[64,128]{1,0:T(8,128)(2,1)}, u32[]{:S(2)}) copy-start(bf16[64,128]{1,0:T(8,128)(2,1)} %param.12) | copy-start | bytes 49156
  82.9 75.1 %copy-start.2 = (bf16[32,256]{1,0:T(8,128)(2,1)S(1)}, bf16[32,256]{1,0:T(8,128)(2,1)}, u32[]{:S(2)}) copy-start(bf16[32,256]{1,0:T(8,128)(2,1)} %param.15) | copy-start | bytes 49156
  159.0 72.9 %all-to-all-start.4 = ((bf16[32,32,256]{2,1,0:T(8,128)(2,1)}), bf16[32,32,256]{2,1,0:T(8,128)(2,1)S(1)}, u32[]{:S(2)}, u32[]{:S(2)}) async-start(bf16[32,32,256]{2,1,0:T(8,128)(2,1)} %broadcast_in_dim.57), calls=%async_computation.4 | async-start | bytes 1048576 | tf_op jit(solution)/shard_map/all_to_all | solution.py:16
  165.2 0.7 copy-start.4
  231.9 28.0 %copy-start.3 = (f32[256]{0:T(256)S(1)}, f32[256]{0:T(256)}, u32[]{:S(2)}) copy-start(f32[256]{0:T(256)} %param.16) | copy-start | bytes 3076
Sparse Core Ops, SparseCore 0:
  9.4 250.1 all-gather.1
where the time goes:
time: 332 us
  blocking collectives  223 us (67%)
  waiting for transfers between devices  65.5 us (20%)
  matrix products  14.9 us (4%)
  between operations  13.7 us (4%)
  local copies, waits for them, and re-layouts  8.26 us (2%)
  starting transfers between devices  5.35 us (2%)
    all_to_all x6, blocking collectives, sent_to_all(): return lax.all_to_all(copies, axis, split_axis=0, concat_axis=0, tiled=True)  198 us
    all_to_all x1, waiting for transfers between devices, sent_to_all(): return lax.all_to_all(copies, axis, split_axis=0, concat_axis=0, tiled=True)  65.4 us
    all_to_all x1, blocking collectives, sum_at_owner(): lax.all_to_all(tiles, axis, split_axis=0, concat_axis=0, tiled=True)  24.1 us
    dot_general x1, matrix products, local(): jnp.einsum('hor,rn->hon', hidden, down_full, preferred_element_type=jnp.f...  8.77 us
  transfers between devices with their start and end apart: 2, of which 1 were waited for; matrix products, arithmetic and copies ran while one was open for 2% of the time, Pallas kernels for 0%

commit v1 on v0

v1 whole, which is shorter than its diff:
```python
import functools

import jax
import jax.numpy as jnp
from jax import lax
from jax.experimental import pallas as pl
from jax.experimental.pallas import tpu as pltpu
from jax.sharding import Mesh
from jax.sharding import PartitionSpec as P

D = 2048
GD = 128
EPSILON = 0.05
CORES = 2
LANES = 128
EXTRA = 16
VM = pltpu.VMEM
F32, BF16 = jnp.float32, jnp.bfloat16


def dot(a, b):
    return lax.dot_general(a, b, (((1,), (0,)), ((), ())), preferred_element_type=F32)


def dot_t(a, b):
    return lax.dot_general(a, b, (((1,), (1,)), ((), ())), preferred_element_type=F32)


def pieces(gain):
    high = lax.reduce_precision(gain, 8, 7)
    rest = gain - high
    mid = lax.reduce_precision(rest, 8, 7)
    return [high, mid, rest - mid]


def gain_row(block, at):
    rows = block[at : at + 3, :].astype(F32)
    return rows[0:1] + rows[1:2] + rows[2:3]


def spec(where=VM):
    return pl.BlockSpec(memory_space=where)


def mixer_kernel(scal, own, other, weight, pool_weight, pool_scale, pooled):
    core, half_width = scal[0], scal[1]
    chips = own.shape[0]
    length, width = own.shape[1] - EXTRA, own.shape[2]
    square = jnp.zeros((length, 1), F32)
    for side in (own, other):
        for chip in range(chips):
            part = side[chip, :length, :].astype(F32)
            square += jnp.sum(part * part, axis=1, keepdims=True)
    scale = lax.rsqrt(square / D + EPSILON)
    total = jnp.zeros((length, weight.shape[1]), F32)
    for which, side in ((core, own), (1 - core, other)):
        for chip in range(chips):
            gain = gain_row(side[chip, length:, :], 0)
            part = side[chip, :length, :].astype(F32)
            normed = (part * scale * gain).astype(BF16)
            row = pl.multiple_of((chip * CORES + which) * width, width)
            total += dot(normed, weight[pl.ds(row, width), :])
    pool_input = total.astype(BF16)
    row = lax.broadcasted_iota(jnp.int32, (length, length), 0)
    column = lax.broadcasted_iota(jnp.int32, (length, length), 1)
    inside = (column >= row - half_width) & (column < row + half_width)
    window = dot(inside.astype(F32).astype(BF16), pool_input)
    at = lax.broadcasted_iota(jnp.int32, (length, 1), 0)
    count = jnp.minimum(at + half_width, length) - jnp.maximum(at - half_width, 0)
    deviation = (window / count.astype(F32) - pool_input.astype(F32)).astype(BF16)
    mapped = dot(deviation, pool_weight[0])
    pooled[...] = (mapped * pool_scale[...]).astype(BF16)


def out_kernel(pooled, weight, tokens, gain, mixed, scaled):
    total = tokens[...].astype(F32)
    depth = pooled.shape[2]
    add = jnp.zeros_like(total)
    for block in range(pooled.shape[0]):
        add += dot(pooled[block], weight[pl.ds(block * depth, depth), :])
    total = total + add
    mixed[...] = total
    scaled[...] = (total * gain[...]).astype(BF16)


def square_kernel(own, other, own_gain, other_gain, scale):
    length = own.shape[1]
    square = jnp.zeros((length, 1), F32)
    for side, gains in ((own, own_gain), (other, other_gain)):
        for chip in range(own.shape[0]):
            gain = gain_row(gains[chip], 3)
            part = side[chip].astype(F32)
            square += jnp.sum(part * part * (1.0 / (gain * gain)), axis=1, keepdims=True)
    scale[...] = jnp.broadcast_to(lax.rsqrt(square / D + EPSILON), scale.shape)


def hidden_kernel(scal, own, other, scale, weight, hidden, partial, wide, down, sems, dsems):
    core = scal[0]
    chips, length, width = own.shape
    blocks = wide.shape[0]

    def gate_copy(i):
        return pltpu.make_async_copy(
            weight.at[:, pl.ds(i * 2 * LANES, 2 * LANES)], wide.at[i], sems.at[i]
        )

    def down_copy(chip):
        row = pl.multiple_of((chip * CORES + 1 - core) * width, width)
        return pltpu.make_async_copy(
            weight.at[pl.ds(row, width), pl.ds(weight.shape[1] - down.shape[2], down.shape[2])],
            down.at[chip],
            dsems.at[chip],
        )

    for i in range(blocks):
        gate_copy(i).start()
    for chip in range(chips):
        down_copy(chip).start()
    factor = scale[...]

    def product(i, columns):
        total = jnp.zeros((length, columns), F32)
        for which, side in ((core, own), (1 - core, other)):
            for chip in range(chips):
                row = pl.multiple_of((chip * CORES + which) * width, width)
                total += dot(side[chip], wide[i, pl.ds(row, width), :columns])
        return total

    def activated(gate, up):
        return (gate / (1.0 + jnp.exp(-gate))) * up

    def full_block(i):
        both = product(i, 2 * LANES)
        return activated(both[:, :LANES] * factor, both[:, LANES:] * factor).astype(BF16)

    def pair(p, carry):
        for j in range(2):
            gate_copy(2 * p + j).wait()
            hidden[p, :, j * LANES : (j + 1) * LANES] = full_block(2 * p + j)
        return carry

    lax.fori_loop(0, blocks // 2 - 1, pair, 0)
    last = blocks // 2 - 1
    gate_copy(blocks - 2).wait()
    hidden[last, :, :LANES] = full_block(blocks - 2)
    gate_copy(blocks - 1).wait()
    both = product(blocks - 1, LANES) * factor
    lane = lax.broadcasted_iota(jnp.int32, both.shape, 1)
    turned = pltpu.roll(both, LANES // 2, 1)
    hidden[last, :, LANES:] = jnp.where(lane < LANES // 2, activated(both, turned), 0.0).astype(BF16)
    for chip in range(chips):
        down_copy(chip).wait()
        total = jnp.zeros((length, width), F32)
        for p in range(blocks // 2):
            total += dot_t(hidden[p], down[chip, :, p * 2 * LANES : (p + 1) * 2 * LANES])
        partial[chip] = total.astype(BF16)


def down_kernel(scal, hidden, weight, partial, down, dsems):
    core = scal[0]
    chips, length, width = partial.shape

    def down_copy(chip):
        row = pl.multiple_of((chip * CORES + core) * width, width)
        return pltpu.make_async_copy(
            weight.at[pl.ds(row, width), pl.ds(weight.shape[1] - down.shape[2], down.shape[2])],
            down.at[chip],
            dsems.at[chip],
        )

    for chip in range(chips):
        down_copy(chip).start()
    for chip in range(chips):
        down_copy(chip).wait()
        total = jnp.zeros((length, width), F32)
        for p in range(hidden.shape[0]):
            total += dot_t(hidden[p], down[chip, :, p * 2 * LANES : (p + 1) * 2 * LANES])
        partial[chip] = total


def call(kernel, outs, flops, moved, in_specs, scratch=()):
    return pl.pallas_call(
        kernel,
        out_shape=outs,
        in_specs=in_specs,
        out_specs=jax.tree.map(lambda _: spec(), outs),
        scratch_shapes=list(scratch),
        cost_estimate=pl.CostEstimate(flops=flops, bytes_accessed=moved, transcendentals=0),
    )


def swap(array):
    return lax.ppermute(array, "core", [(0, 1), (1, 0)])


def local(
    tokens,
    norm_gain,
    in_weight,
    pool_weight,
    pool_scale,
    out_weight,
    ffn_gain,
    gate_weight,
    up_weight,
    down_weight,
):
    _, length, width = tokens.shape
    rows, units = gate_weight.shape
    core = lax.axis_index("core")
    chips = lax.axis_size("x")
    group = lax.axis_index("x") * CORES + core
    scal = jnp.stack([core, jnp.left_shift(1, group % 4)]).astype(jnp.int32)
    smem = spec(pltpu.SMEM)

    whole = units // LANES
    columns = []
    for i in range(whole):
        columns += [a[:, i * LANES : (i + 1) * LANES] for a in (gate_weight, up_weight)]
    columns += [a[:, whole * LANES :] for a in (gate_weight, up_weight)]
    columns += [down_weight.T, jnp.zeros((rows, LANES - units % LANES), BF16)]
    weight = lax.all_gather(jnp.concatenate(columns, axis=1), "fs", axis=0, tiled=True)

    gains = jnp.stack(pieces(norm_gain) + pieces(ffn_gain)).astype(BF16)
    sent = jnp.concatenate(
        [tokens[0], gains, jnp.zeros((EXTRA - gains.shape[0], width), BF16)], axis=0
    )
    own = lax.all_gather(sent, "x", axis=0)
    other = swap(own)
    in_full = lax.all_gather(in_weight, "fs", axis=0, tiled=True)
    out_full = lax.all_gather(out_weight, "fs", axis=0, tiled=True)
    channels = in_full.shape[1]
    pooled = call(
        mixer_kernel,
        jax.ShapeDtypeStruct((length, channels), BF16),
        2 * length * D * channels,
        6 * length * D,
        [smem] + [spec()] * 5,
    )(scal, own, other, in_full, pool_weight, pool_scale.reshape(1, -1))
    pooled_all = lax.all_gather(pooled, ("x", "core"), axis=0)
    mixed, scaled = call(
        out_kernel,
        (
            jax.ShapeDtypeStruct((length, width), F32),
            jax.ShapeDtypeStruct((length, width), BF16),
        ),
        2 * length * width * out_full.shape[0],
        4 * length * D,
        [spec()] * 4,
    )(pooled_all, out_full, tokens[0], ffn_gain.reshape(1, -1))
    own_two = lax.all_gather(scaled, "x", axis=0)
    other_two = swap(own_two)
    scale_two = call(
        square_kernel,
        jax.ShapeDtypeStruct((length, LANES), F32),
        6 * length * D,
        2 * length * D,
        [spec()] * 4,
    )(own_two, other_two, own[:, length:], other[:, length:])

    blocks = (units + LANES - 1) // LANES
    depth = blocks * LANES
    down_scratch = (
        VM((chips, width, depth), BF16),
        pltpu.SemaphoreType.DMA((chips,)),
    )
    anywhere = spec(pl.ANY)
    hidden, partial_other = call(
        hidden_kernel,
        (
            jax.ShapeDtypeStruct((blocks // 2, length, 2 * LANES), BF16),
            jax.ShapeDtypeStruct((chips, length, width), BF16),
        ),
        5 * length * D * units,
        4 * D * units,
        [smem, spec(), spec(), spec(), anywhere],
        (
            VM((blocks, D, 2 * LANES), BF16),
            down_scratch[0],
            pltpu.SemaphoreType.DMA((blocks,)),
            down_scratch[1],
        ),
    )(scal, own_two, other_two, scale_two, weight)
    arrived = swap(partial_other)
    partial_own = call(
        down_kernel,
        jax.ShapeDtypeStruct((chips, length, width), F32),
        length * D * units,
        D * units,
        [smem, spec(), anywhere],
        down_scratch,
    )(scal, hidden, weight)
    paired = (partial_own + arrived.astype(F32)).astype(BF16)
    summed = lax.all_to_all(paired, "x", split_axis=0, concat_axis=0, tiled=True)
    return (mixed + summed.astype(F32).sum(axis=0)).astype(BF16)[None]


def solution(mesh):
    sizes = mesh.devices.shape
    fine = Mesh(
        mesh.devices.reshape(*sizes[:2], sizes[2] // CORES, CORES), ("grp", "fs", "x", "core")
    )
    tp = ("x", "core")
    return jax.shard_map(
        local,
        mesh=fine,
        in_specs=(
            P(("grp", "fs"), None, tp),
            P(tp),
            P("fs", tp),
            P(tp, None, None),
            P(tp),
            P("fs", tp),
            P(tp),
            P("fs", tp),
            P("fs", tp),
            P(tp, "fs"),
        ),
        out_specs=P(("grp", "fs"), None, tp),
        check_vma=False,
    )
```

time: 332 us -> 287 us (0.86)
  waiting for transfers between devices: 65.5 us -> 0.06 us
  starting transfers between devices: 5.35 us -> 50.6 us
  blocking collectives: 223 us -> 182 us
  Pallas kernels: 0 us -> 25.5 us
  matrix products: 14.9 us -> 0 us
    all_to_all x7 -> x1, blocking collectives: 223 us -> 15.8 us  [local(): lax.all_to_all(paired, 'x', split_axis=0, concat_axis=0, tiled=True)]
    all_gather x0 -> x5, blocking collectives: none -> 166 us  [the longest x1 54.7 us: local(): in_full = lax.all_gather(in_weight, 'fs', axis=0, tiled=True)]
    all_to_all x1 -> x0, waiting for transfers between devices: 65.4 us -> none  [sent_to_all(): return lax.all_to_all(copies, axis, split_axis=0, concat_axis=0, tiled=True)]
    ppermute x0 -> x3, starting transfers between devices: none -> 50.6 us  [swap(): return lax.ppermute(array, 'core', [(0, 1), (1, 0)])]
    pallas_call x0 -> x5, Pallas kernels: none -> 25.5 us  [the longest x1 11.5 us: local(): call(hidden_kernel, (jax.ShapeDtypeStruct((blocks // 2, length, 2 * LANES...]
    dot_general x5 -> x0, matrix products: 14.9 us -> none  [the longest x1 8.77 us: local(): jnp.einsum('hor,rn->hon', hidden, down_full, preferred_element_type=jnp.f...]
    all_to_all x1 -> x0, starting transfers between devices: 5.35 us -> none  [sent_to_all(): return lax.all_to_all(copies, axis, split_axis=0, concat_axis=0, tiled=True)]
    slice x5, local copies, waits for them, and re-layouts: 0.11 us -> 5.05 us  [the longest x2 1.45 us: local(): columns += [a[:, whole * LANES:] for a in (gate_weight, up_weight)]]
  transfers between devices with their start and end apart: 2 -> 4, of which waited for: 1 -> 0; matrix products, arithmetic and copies ran while one was open for 2% -> 2% of each run, Pallas kernels for 0% -> 5%
where the time goes in v1:
time: 287 us; the launch traced here: 286 us
  blocking collectives  182 us (63%)
  starting transfers between devices  50.6 us (18%)
  Pallas kernels  25.5 us (9%)
  between operations  13.6 us (5%)
  local copies, waits for them, and re-layouts  9.69 us (3%)
  other arithmetic  4.38 us (2%)
    all_gather x1, blocking collectives, local(): in_full = lax.all_gather(in_weight, 'fs', axis=0, tiled=True)  54.7 us
    all_gather x1, blocking collectives, local(): out_full = lax.all_gather(out_weight, 'fs', axis=0, tiled=True)  51.8 us
    ppermute x3, starting transfers between devices, swap(): return lax.ppermute(array, 'core', [(0, 1), (1, 0)])  50.6 us
    all_gather x1, blocking collectives, local(): pooled_all = lax.all_gather(pooled, ('x', 'core'), axis=0)  35.2 us
    all_to_all x1, blocking collectives, local(): lax.all_to_all(paired, 'x', split_axis=0, concat_axis=0, tiled=True)  15.8 us
    all_gather x1, blocking collectives, local(): own_two = lax.all_gather(scaled, 'x', axis=0)  12.4 us
    all_gather x1, blocking collectives, local(): own = lax.all_gather(sent, 'x', axis=0)  12 us
    pallas_call x1, Pallas kernels, local(): call(hidden_kernel, (jax.ShapeDtypeStruct((blocks // 2, length, 2 * LANES...  11.5 us
  transfers between devices with their start and end apart: 4, of which 0 were waited for; matrix products, arithmetic and copies ran while one was open for 2% of the time, Pallas kernels for 5%

profile of v1, /device:TPU:33, one launch (start us, length us, event | category | flops | bytes accessed | tf_op | source)
XLA Modules:
  0.0 285.7 jit_solution(9691614827099364001)
XLA Ops:
  6.6 0.7 slice.54
  7.3 0.7 slice.55
  8.0 0.9 fusion.3
  8.9 1.7 concatenate.8
  12.1 1.1 concatenate.7
  13.2 12.0 %all-gather = bf16[1600,256]{1,0:T(8,128)(2,1)S(1)} all-gather(bf16[400,256]{1,0:T(8,128)(2,1)S(1)} %concatenate.7), channel_id=2, replica_groups=mesh['grp'=2,'fs'=32,'x'=4,'core'=2] {'x'}, dimensions={0}, use_global_device_ids=true | all-gather | bytes 1024000 | tf_op jit(solution)/shard_map/all_gather | solution.py:228
  25.2 44.8 %collective-permute-start = (bf16[4,400,256]{2,1,0:T(8,128)(2,1)S(1)}, bf16[4,400,256]{2,1,0:T(8,128)(2,1)S(1)}, u32[]{:S(2)}, u32[]{:S(2)}) collective-permute-start(bf16[4,400,256]{2,1,0:T(8,128)(2,1)S(1)} %bitcast.14), channel_id=1, source_target_pairs={{0,1},{1,0},{2,3},{3,2},{4,5},{5,4},{6,7},{7,6},{8,9},{9,8},{10,11... | collective-permute-start | bytes 2457608 | tf_op jit(solution)/shard_map/ppermute | solution.py:193
  70.6 54.7 %all_gather.29.weight = bf16[2048,128]{1,0:T(8,128)(2,1)} all-gather(bf16[64,128]{1,0:T(8,128)(2,1)S(1)} %copy-done.5), channel_id=1, replica_groups=mesh['grp'=2,'fs'=32,'x'=4,'core'=2] {'fs'}, dimensions={0}, use_global_device_ids=true | all-gather | bytes 540672 | tf_op jit(solution)/shard_map/all_gather | solution.py:230
  125.4 51.8 %all_gather.32.weight = bf16[1024,256]{1,0:T(8,128)(2,1)} all-gather(bf16[32,256]{1,0:T(8,128)(2,1)S(1)} %copy-done.6), channel_id=1, replica_groups=mesh['grp'=2,'fs'=32,'x'=4,'core'=2] {'fs'}, dimensions={0}, use_global_device_ids=true | all-gather | bytes 540672 | tf_op jit(solution)/shard_map/all_gather | solution.py:231
  177.2 0.9 copy-done.3
  178.1 3.6 %shard_map.100 = bf16[384,128]{1,0:T(8,128)(2,1)} custom-call(s32[2]{0:T(128)} %pad_add_fusion.scal, bf16[4,400,256]{2,1,0:T(8,128)(2,1)} %bitcast.15, bf16[4,400,256]{2,1,0:T(8,128)(2,1)} %copy-done.3, bf16[2048,128]{1,0:T(8,128)(2,1)} %all_gather.29.weight, bf16[1,128,128]{2,1,0:T(8,128)(2,1)} %pool_weight.1, f32[1,128]{1,0:T(1,128)} %bitcast.22), custom_call_target="tpu_custom_call" | custom-call | flops 201326592 | bytes 4718592 | tf_op jit(solution)/shard_map/pallas_call | solution.py:233
  181.7 35.2 %all-gather.1 = bf16[3072,128]{1,0:T(8,128)(2,1)} all-gather(bf16[384,128]{1,0:T(8,128)(2,1)} %shard_map.100), channel_id=3, replica_groups=mesh['grp'=2,'fs'=32,'x'=4,'core'=2] {'x','core'}, dimensions={0}, use_global_device_ids=true | all-gather | bytes 884736 | tf_op jit(solution)/shard_map/all_gather | solution.py:240
  216.9 2.7 shard_map.101
  219.6 12.4 %all-gather.2 = bf16[1536,256]{1,0:T(8,128)(2,1)S(1)} all-gather(bf16[384,256]{1,0:T(8,128)(2,1)} %get-tuple-element.10), channel_id=4, replica_groups=mesh['grp'=2,'fs'=32,'x'=4,'core'=2] {'x'}, dimensions={0}, use_global_device_ids=true | all-gather | bytes 983040 | tf_op jit(solution)/shard_map/all_gather | solution.py:251
  232.0 3.8 %collective-permute-start.1 = (bf16[4,384,256]{2,1,0:T(8,128)(2,1)S(1)}, bf16[4,384,256]{2,1,0:T(8,128)(2,1)S(1)}, u32[]{:S(2)}, u32[]{:S(2)}) collective-permute-start(bf16[4,384,256]{2,1,0:T(8,128)(2,1)S(1)} %bitcast.11), channel_id=1, source_target_pairs={{0,1},{1,0},{2,3},{3,2},{4,5},{5,4},{6,7},{7,6},{8,9},{9,8},{10,11... | collective-permute-start | bytes 2359304 | tf_op jit(solution)/shard_map/ppermute | solution.py:193
  235.8 1.4 slice.56.own_gain
  237.2 1.4 slice.57.other_gain
  238.6 0.9 copy-done.2
  239.5 2.6 shard_map.102.scale
  242.0 11.5 %shard_map.103 = (bf16[3,384,256]{2,1,0:T(8,128)(2,1)}, bf16[4,384,256]{2,1,0:T(8,128)(2,1)}) custom-call(s32[2]{0:T(128)} %pad_add_fusion.scal, bf16[4,384,256]{2,1,0:T(8,128)(2,1)} %bitcast.13, bf16[4,384,256]{2,1,0:T(8,128)(2,1)} %copy-done.2, f32[384,128]{1,0:T(8,128)} %shard_map.102.scale, bf16[2048,2176]{1,0:T(8,128)(2,1)} %all-gather.5.cloned.1.call-done.weight), custom_call_target="tpu_custom_call" | custom-call | flops 2768240640 | bytes 5767168 | tf_op jit(solution)/shard_map/pallas_call | solution.py:268
  253.5 2.0 collective-permute-start.2
  255.4 5.2 %shard_map.104 = f32[4,384,256]{2,1,0:T(8,128)} custom-call(s32[2]{0:T(128)} %pad_add_fusion.scal, bf16[3,384,256]{2,1,0:T(8,128)(2,1)} %get-tuple-element.11.hidden, bf16[2048,2176]{1,0:T(8,128)(2,1)} %all-gather.5.cloned.1.call-done.weight), custom_call_target="tpu_custom_call" | custom-call | flops 553648128 | bytes 1441792 | tf_op jit(solution)/shard_map/pallas_call | solution.py:285
  260.7 1.6 add_convert_fusion
  262.3 15.8 %all_to_all.5 = bf16[4,384,256]{2,1,0:T(8,128)(2,1)S(1)} all-to-all(bf16[4,384,256]{2,1,0:T(8,128)(2,1)S(1)} %add_convert_fusion), channel_id=1, replica_groups=mesh['grp'=2,'fs'=32,'x'=4,'core'=2] {'x'}, dimensions={0} | all-to-all | bytes 1572864 | tf_op jit(solution)/shard_map/all_to_all | solution.py:294
  (31 shorter events, 2.9 us)
Async XLA Ops:
  6.5 64.1 %copy-start.5 = (bf16[64,128]{1,0:T(8,128)(2,1)S(1)}, bf16[64,128]{1,0:T(8,128)(2,1)}, u32[]{:S(2)}) copy-start(bf16[64,128]{1,0:T(8,128)(2,1)} %param.12) | copy-start | bytes 49156
  6.5 235.5 %all-gather.5.cloned.1.call-start = ((), (), s32[]{:S(2)}) async-start(), calls=%async_computation.1 | async-start | bytes 9191424 | tf_op jit(solution)/shard_map/all_gather | solution.py:222
  8.0 117.4 %copy-start.6 = (bf16[32,256]{1,0:T(8,128)(2,1)S(1)}, bf16[32,256]{1,0:T(8,128)(2,1)}, u32[]{:S(2)}) copy-start(bf16[32,256]{1,0:T(8,128)(2,1)} %param.15) | copy-start | bytes 49156
  25.2 152.0 %copy-start.1 = (bf16[1600,256]{1,0:T(8,128)(2,1)}, bf16[1600,256]{1,0:T(8,128)(2,1)S(1)}, u32[]{:S(2)}) copy-start(bf16[1600,256]{1,0:T(8,128)(2,1)S(1)} %all-gather) | copy-start | bytes 2457604
  25.2 152.0 %collective-permute-start = (bf16[4,400,256]{2,1,0:T(8,128)(2,1)S(1)}, bf16[4,400,256]{2,1,0:T(8,128)(2,1)S(1)}, u32[]{:S(2)}, u32[]{:S(2)}) collective-permute-start(bf16[4,400,256]{2,1,0:T(8,128)(2,1)S(1)} %bitcast.14), channel_id=1, source_target_pairs={{0,1},{1,0},{2,3},{3,2},{4,5},{5,4},{6,7},{7,6},{8,9},{9,8},{10,11... | collective-permute-start | bytes 2457608 | tf_op jit(solution)/shard_map/ppermute | solution.py:193
  177.2 0.9 copy-start.3
  232.0 6.6 %copy-start = (bf16[1536,256]{1,0:T(8,128)(2,1)}, bf16[1536,256]{1,0:T(8,128)(2,1)S(1)}, u32[]{:S(2)}) copy-start(bf16[1536,256]{1,0:T(8,128)(2,1)S(1)} %all-gather.2) | copy-start | bytes 2359300
  232.0 6.6 %collective-permute-start.1 = (bf16[4,384,256]{2,1,0:T(8,128)(2,1)S(1)}, bf16[4,384,256]{2,1,0:T(8,128)(2,1)S(1)}, u32[]{:S(2)}, u32[]{:S(2)}) collective-permute-start(bf16[4,384,256]{2,1,0:T(8,128)(2,1)S(1)} %bitcast.11), channel_id=1, source_target_pairs={{0,1},{1,0},{2,3},{3,2},{4,5},{5,4},{6,7},{7,6},{8,9},{9,8},{10,11... | collective-permute-start | bytes 2359304 | tf_op jit(solution)/shard_map/ppermute | solution.py:193
  238.6 0.9 copy-start.2
  253.5 7.2 %collective-permute-start.2 = (bf16[4,384,256]{2,1,0:T(8,128)(2,1)}, bf16[4,384,256]{2,1,0:T(8,128)(2,1)S(1)}, u32[]{:S(2)}, u32[]{:S(2)}) collective-permute-start(bf16[4,384,256]{2,1,0:T(8,128)(2,1)} %get-tuple-element.12), channel_id=1, source_target_pairs={{0,1},{1,0},{2,3},{3,2},{4,5},{5,4},{6,7},{7,6},{8,9},{9,8},{10,11... | collective-permute-start | bytes 2359304 | tf_op jit(solution)/shard_map/ppermute | solution.py:193
  262.3 15.9 %copy-start.4 = (f32[384,256]{1,0:T(8,128)S(1)}, f32[384,256]{1,0:T(8,128)}, u32[]{:S(2)}) copy-start(f32[384,256]{1,0:T(8,128)} %get-tuple-element.9) | copy-start | bytes 1179652
Sparse Core Ops, SparseCore 0:
  10.8 164.9 all-gather.4

commit v2 on v1

--- a/solution.py
+++ b/solution.py
@@ -1,5 +1,3 @@
-import functools
-
 import jax
 import jax.numpy as jnp
 from jax import lax
@@ -26,11 +24,39 @@
     return lax.dot_general(a, b, (((1,), (1,)), ((), ())), preferred_element_type=F32)
 
 
-def pieces(gain):
-    high = lax.reduce_precision(gain, 8, 7)
-    rest = gain - high
-    mid = lax.reduce_precision(rest, 8, 7)
-    return [high, mid, rest - mid]
+def pack_kernel(*refs):
+    count = 6
+    weight, sent, sems = refs[count], refs[count + 1], refs[-1]
+    copies = [
+        pltpu.make_async_copy(source, target, sems.at[i])
+        for i, (source, target) in enumerate(zip(refs[:count], refs[count + 2 : -1]))
+    ]
+    for copy in copies:
+        copy.start()
+    for copy in copies:
+        copy.wait()
+    tokens, norm_gain, ffn_gain, gate, up, down = refs[count + 2 : -1]
+    units = gate.shape[1]
+    whole = units // LANES
+    for i in range(whole):
+        weight[:, 2 * i * LANES : (2 * i + 1) * LANES] = gate[:, i * LANES : (i + 1) * LANES]
+        weight[:, (2 * i + 1) * LANES : (2 * i + 2) * LANES] = up[:, i * LANES : (i + 1) * LANES]
+    at = 2 * units
+    weight[:, 2 * whole * LANES : at] = jnp.concatenate(
+        [gate[:, whole * LANES :], up[:, whole * LANES :]], axis=1
+    )
+    weight[:, at : at + whole * LANES] = down[:, : whole * LANES]
+    rest = down[:, whole * LANES :]
+    weight[:, at + whole * LANES :] = jnp.concatenate([rest, jnp.zeros_like(rest)], axis=1)
+    length = tokens.shape[0]
+    sent[:length, :] = tokens[...]
+    rows = []
+    for gain in (norm_gain[...], ffn_gain[...]):
+        high = gain.astype(BF16).astype(F32)
+        mid = (gain - high).astype(BF16).astype(F32)
+        rows += [high, mid, gain - high - mid]
+    rows.append(jnp.zeros((EXTRA - len(rows), tokens.shape[1]), F32))
+    sent[length:, :] = jnp.concatenate(rows, axis=0).astype(BF16)
 
 
 def gain_row(block, at):
@@ -42,8 +68,17 @@
     return pl.BlockSpec(memory_space=where)
 
 
-def mixer_kernel(scal, own, other, weight, pool_weight, pool_scale, pooled):
+def mixer_kernel(scal, own, other, mine, theirs, pool_weight, pool_scale, pooled, weight):
     core, half_width = scal[0], scal[1]
+
+    @pl.when(scal[2] == 0)
+    def _():
+        weight[...] = mine[...]
+
+    @pl.when(scal[2] != 0)
+    def _():
+        weight[...] = theirs[...]
+
     chips = own.shape[0]
     length, width = own.shape[1] - EXTRA, own.shape[2]
     square = jnp.zeros((length, 1), F32)
@@ -72,31 +107,50 @@
     pooled[...] = (mapped * pool_scale[...]).astype(BF16)
 
 
-def out_kernel(pooled, weight, tokens, gain, mixed, scaled):
-    total = tokens[...].astype(F32)
-    depth = pooled.shape[2]
-    add = jnp.zeros_like(total)
-    for block in range(pooled.shape[0]):
-        add += dot(pooled[block], weight[pl.ds(block * depth, depth), :])
-    total = total + add
+def out_kernel(scal, pooled, mine, theirs, tokens, gain, mixed, scaled, weight):
+    half = tokens.shape[1] // 2
+    blocks, _, depth = pooled.shape
+    shard = mine.shape[1] // 2
+
+    def lay(source):
+        for side in range(2):
+            rows = source[:, side * shard : (side + 1) * shard, :]
+            weight[:, side * half : (side + 1) * half] = rows.reshape(-1, half)
+
+    @pl.when(scal[2] == 0)
+    def _():
+        lay(theirs)
+
+    @pl.when(scal[2] != 0)
+    def _():
+        lay(mine)
+
+    add = jnp.zeros(tokens.shape, F32)
+    for block in range(blocks):
+        add += dot(pooled[block], weight[block * depth : (block + 1) * depth, :])
+    total = tokens[...].astype(F32) + add
     mixed[...] = total
     scaled[...] = (total * gain[...]).astype(BF16)
 
 
-def square_kernel(own, other, own_gain, other_gain, scale):
-    length = own.shape[1]
+def square_kernel(scal, own, other, own_gain, other_gain, scale, features):
+    core = scal[0]
+    chips, length, width = own.shape
     square = jnp.zeros((length, 1), F32)
-    for side, gains in ((own, own_gain), (other, other_gain)):
-        for chip in range(own.shape[0]):
-            gain = gain_row(gains[chip], 3)
-            part = side[chip].astype(F32)
+    for which, side, gains in ((core, own, own_gain), (1 - core, other, other_gain)):
+        for chip in range(chips):
+            gain = gain_row(gains[chip, length:, :], 3)
+            block = side[chip]
+            column = pl.multiple_of((chip * CORES + which) * width, width)
+            features[:, pl.ds(column, width)] = block
+            part = block.astype(F32)
             square += jnp.sum(part * part * (1.0 / (gain * gain)), axis=1, keepdims=True)
     scale[...] = jnp.broadcast_to(lax.rsqrt(square / D + EPSILON), scale.shape)
 
 
-def hidden_kernel(scal, own, other, scale, weight, hidden, partial, wide, down, sems, dsems):
+def hidden_kernel(scal, features_at, scale, weight, hidden, partial, features, wide, down, sems, dsems):
     core = scal[0]
-    chips, length, width = own.shape
+    chips, length, width = partial.shape
     blocks = wide.shape[0]
 
     def gate_copy(i):
@@ -112,19 +166,17 @@
             dsems.at[chip],
         )
 
+    feature_copy = pltpu.make_async_copy(features_at, features, sems.at[blocks])
+    feature_copy.start()
     for i in range(blocks):
         gate_copy(i).start()
     for chip in range(chips):
         down_copy(chip).start()
     factor = scale[...]
+    feature_copy.wait()
 
     def product(i, columns):
-        total = jnp.zeros((length, columns), F32)
-        for which, side in ((core, own), (1 - core, other)):
-            for chip in range(chips):
-                row = pl.multiple_of((chip * CORES + which) * width, width)
-                total += dot(side[chip], wide[i, pl.ds(row, width), :columns])
-        return total
+        return dot(features[...], wide[i, :, :columns])
 
     def activated(gate, up):
         return (gate / (1.0 + jnp.exp(-gate))) * up
@@ -178,13 +230,14 @@
         partial[chip] = total
 
 
-def call(kernel, outs, flops, moved, in_specs, scratch=()):
+def call(kernel, outs, flops, moved, in_specs, scratch=(), vmem=12):
     return pl.pallas_call(
         kernel,
         out_shape=outs,
         in_specs=in_specs,
         out_specs=jax.tree.map(lambda _: spec(), outs),
         scratch_shapes=list(scratch),
+        compiler_params=pltpu.CompilerParams(vmem_limit_bytes=vmem << 20),
         cost_estimate=pl.CostEstimate(flops=flops, bytes_accessed=moved, transcendentals=0),
     )
 
@@ -210,61 +263,89 @@
     core = lax.axis_index("core")
     chips = lax.axis_size("x")
     group = lax.axis_index("x") * CORES + core
-    scal = jnp.stack([core, jnp.left_shift(1, group % 4)]).astype(jnp.int32)
+    partner = lax.axis_index("grp") % 2
+    scal = jnp.stack([core, jnp.left_shift(1, group % 4), partner]).astype(jnp.int32)
     smem = spec(pltpu.SMEM)
-
-    whole = units // LANES
-    columns = []
-    for i in range(whole):
-        columns += [a[:, i * LANES : (i + 1) * LANES] for a in (gate_weight, up_weight)]
-    columns += [a[:, whole * LANES :] for a in (gate_weight, up_weight)]
-    columns += [down_weight.T, jnp.zeros((rows, LANES - units % LANES), BF16)]
-    weight = lax.all_gather(jnp.concatenate(columns, axis=1), "fs", axis=0, tiled=True)
-
-    gains = jnp.stack(pieces(norm_gain) + pieces(ffn_gain)).astype(BF16)
-    sent = jnp.concatenate(
-        [tokens[0], gains, jnp.zeros((EXTRA - gains.shape[0], width), BF16)], axis=0
-    )
+    anywhere = spec(pl.ANY)
+    blocks = (units + LANES - 1) // LANES
+    depth = blocks * LANES
+
+    unpacked = (
+        tokens[0],
+        norm_gain.reshape(1, -1),
+        ffn_gain.reshape(1, -1),
+        gate_weight,
+        up_weight,
+        down_weight.T,
+    )
+    packed, sent = call(
+        pack_kernel,
+        (
+            jax.ShapeDtypeStruct((rows, 2 * units + depth), BF16),
+            jax.ShapeDtypeStruct((length + EXTRA, width), BF16),
+        ),
+        0,
+        8 * rows * units,
+        [anywhere] * 6,
+        [VM(a.shape, a.dtype) for a in unpacked] + [pltpu.SemaphoreType.DMA((6,))],
+        63,
+    )(*unpacked)
+    weight = lax.all_gather(packed, "fs", axis=0, tiled=True)
+
     own = lax.all_gather(sent, "x", axis=0)
     other = swap(own)
-    in_full = lax.all_gather(in_weight, "fs", axis=0, tiled=True)
-    out_full = lax.all_gather(out_weight, "fs", axis=0, tiled=True)
-    channels = in_full.shape[1]
+
+    channels = in_weight.shape[1]
+    out_turned = jnp.concatenate(jnp.split(out_weight, width // channels, axis=1), axis=0)
+    chosen = jnp.where(partner == 0, in_weight, out_turned)
+    mine = lax.all_gather(chosen, "fs", axis=0, tiled=True)
+    groups = lax.axis_size("grp")
+    theirs = lax.ppermute(mine, "grp", [(i, i ^ 1) for i in range(groups)])
     pooled = call(
         mixer_kernel,
         jax.ShapeDtypeStruct((length, channels), BF16),
         2 * length * D * channels,
         6 * length * D,
-        [smem] + [spec()] * 5,
-    )(scal, own, other, in_full, pool_weight, pool_scale.reshape(1, -1))
+        [smem] + [spec()] * 6,
+        (VM(mine.shape, BF16),),
+    )(scal, own, other, mine, theirs, pool_weight, pool_scale.reshape(1, -1))
     pooled_all = lax.all_gather(pooled, ("x", "core"), axis=0)
+    by_shard = (-1, out_turned.shape[0], channels)
     mixed, scaled = call(
         out_kernel,
         (
             jax.ShapeDtypeStruct((length, width), F32),
             jax.ShapeDtypeStruct((length, width), BF16),
         ),
-        2 * length * width * out_full.shape[0],
+        2 * length * width * pooled_all.shape[0] * channels,
         4 * length * D,
-        [spec()] * 4,
-    )(pooled_all, out_full, tokens[0], ffn_gain.reshape(1, -1))
+        [smem] + [spec()] * 5,
+        (VM((pooled_all.shape[0] * channels, width), BF16),),
+    )(
+        scal,
+        pooled_all,
+        mine.reshape(by_shard),
+        theirs.reshape(by_shard),
+        tokens[0],
+        ffn_gain.reshape(1, -1),
+    )
     own_two = lax.all_gather(scaled, "x", axis=0)
     other_two = swap(own_two)
-    scale_two = call(
+    scale_two, features = call(
         square_kernel,
-        jax.ShapeDtypeStruct((length, LANES), F32),
+        (
+            jax.ShapeDtypeStruct((length, LANES), F32),
+            jax.ShapeDtypeStruct((length, chips * CORES * width), BF16),
+        ),
         6 * length * D,
-        2 * length * D,
-        [spec()] * 4,
-    )(own_two, other_two, own[:, length:], other[:, length:])
-
-    blocks = (units + LANES - 1) // LANES
-    depth = blocks * LANES
+        4 * length * D,
+        [smem] + [spec()] * 4,
+    )(scal, own_two, other_two, own, other)
+
     down_scratch = (
         VM((chips, width, depth), BF16),
         pltpu.SemaphoreType.DMA((chips,)),
     )
-    anywhere = spec(pl.ANY)
     hidden, partial_other = call(
         hidden_kernel,
         (
@@ -273,14 +354,16 @@
         ),
         5 * length * D * units,
         4 * D * units,
-        [smem, spec(), spec(), spec(), anywhere],
+        [smem, anywhere, spec(), anywhere],
         (
+            VM(features.shape, BF16),
             VM((blocks, D, 2 * LANES), BF16),
             down_scratch[0],
-            pltpu.SemaphoreType.DMA((blocks,)),
+            pltpu.SemaphoreType.DMA((blocks + 1,)),
             down_scratch[1],
         ),
-    )(scal, own_two, other_two, scale_two, weight)
+        56,
+    )(scal, features, scale_two, weight)
     arrived = swap(partial_other)
     partial_own = call(
         down_kernel,
@@ -289,6 +372,7 @@
         D * units,
         [smem, spec(), anywhere],
         down_scratch,
+        56,
     )(scal, hidden, weight)
     paired = (partial_own + arrived.astype(F32)).astype(BF16)
     summed = lax.all_to_all(paired, "x", split_axis=0, concat_axis=0, tiled=True)

time: 287 us -> 233 us (0.81)
  blocking collectives: 182 us -> 115 us
  starting transfers between devices: 50.6 us -> 67.8 us
  waiting for transfers between devices: 0.06 us -> 8.81 us
  local copies, waits for them, and re-layouts: 9.69 us -> 1.85 us
    all_gather x2 -> x1, blocking collectives: 107 us -> 51.2 us  [local(): mine = lax.all_gather(chosen, 'fs', axis=0, tiled=True)]
    ppermute x3, starting transfers between devices: 50.6 us -> 63.6 us  [swap(): return lax.ppermute(array, 'core', [(0, 1), (1, 0)])]
    all_gather x1, blocking collectives: 35.2 us -> 23.3 us  [local(): pooled_all = lax.all_gather(pooled, ('x', 'core'), axis=0)]
    ppermute x0 -> x1, waiting for transfers between devices: none -> 6.86 us  [local(): theirs = lax.ppermute(mine, 'grp', [(i, i ^ 1) for i in range(groups)])]
    slice x5 -> x0, local copies, waits for them, and re-layouts: 5.05 us -> none  [the longest x2 1.45 us: local(): columns += [a[:, whole * LANES:] for a in (gate_weight, up_weight)]]
    ppermute x0 -> x1, starting transfers between devices: none -> 4.13 us  [local(): theirs = lax.ppermute(mine, 'grp', [(i, i ^ 1) for i in range(groups)])]
  transfers between devices with their start and end apart: 4 -> 5, of which waited for: 0 -> 2; matrix products, arithmetic and copies ran while one was open for 2% -> 0% of each run, Pallas kernels for 5% -> 4%
where the time goes in v2:
time: 233 us
  blocking collectives  115 us (49%)
  starting transfers between devices  67.8 us (29%)
  Pallas kernels  23 us (10%)
  between operations  13.6 us (6%)
  waiting for transfers between devices  8.81 us (4%)
  other arithmetic  2.5 us (1%)
    ppermute x3, starting transfers between devices, swap(): return lax.ppermute(array, 'core', [(0, 1), (1, 0)])  63.6 us
    all_gather x1, blocking collectives, local(): mine = lax.all_gather(chosen, 'fs', axis=0, tiled=True)  51.2 us
    all_gather x1, blocking collectives, local(): pooled_all = lax.all_gather(pooled, ('x', 'core'), axis=0)  23.3 us
    all_to_all x1, blocking collectives, local(): lax.all_to_all(paired, 'x', split_axis=0, concat_axis=0, tiled=True)  16.1 us
    all_gather x1, blocking collectives, local(): own_two = lax.all_gather(scaled, 'x', axis=0)  12.4 us
    all_gather x1, blocking collectives, local(): own = lax.all_gather(sent, 'x', axis=0)  12.2 us
    pallas_call x1, Pallas kernels, local(): call(hidden_kernel, (jax.ShapeDtypeStruct((blocks // 2, length, 2 * LANES...  11.5 us
    ppermute x1, waiting for transfers between devices, local(): theirs = lax.ppermute(mine, 'grp', [(i, i ^ 1) for i in range(groups)])  6.86 us
  transfers between devices with their start and end apart: 5, of which 2 were waited for; matrix products, arithmetic and copies ran while one was open for 0% of the time, Pallas kernels for 4%

profile of v2, /device:TPU:33, one launch (start us, length us, event | category | flops | bytes accessed | tf_op | source)
XLA Modules:
  0.0 232.7 jit_solution(6805537589507480973)
XLA Ops:
  6.6 0.1 all-gather.5.cloned.1.call-start
  6.6 2.0 shard_map.100
  8.7 12.2 %all-gather = bf16[1600,256]{1,0:T(8,128)(2,1)S(1)} all-gather(bf16[400,256]{1,0:T(8,128)(2,1)} %get-tuple-element.13), channel_id=2, replica_groups=mesh['grp'=2,'fs'=32,'x'=4,'core'=2] {'x'}, dimensions={0}, use_global_device_ids=true | all-gather | bytes 1024000 | tf_op jit(solution)/shard_map/all_gather | solution.py:295
  20.9 44.8 %collective-permute-start = (bf16[4,400,256]{2,1,0:T(8,128)(2,1)S(1)}, bf16[4,400,256]{2,1,0:T(8,128)(2,1)S(1)}, u32[]{:S(2)}, u32[]{:S(2)}) collective-permute-start(bf16[4,400,256]{2,1,0:T(8,128)(2,1)S(1)} %bitcast.15), channel_id=1, source_target_pairs={{0,1},{1,0},{2,3},{3,2},{4,5},{5,4},{6,7},{7,6},{8,9},{9,8},{10,11... | collective-permute-start | bytes 2457608 | tf_op jit(solution)/shard_map/ppermute | solution.py:246
  65.8 51.2 %all_gather.26.mine = bf16[2048,128]{1,0:T(8,128)(2,1)S(1)} all-gather(bf16[64,128]{1,0:T(8,128)(2,1)S(1)} %maximum_select_fusion), channel_id=1, replica_groups=mesh['grp'=2,'fs'=32,'x'=4,'core'=2] {'fs'}, dimensions={0}, use_global_device_ids=true | all-gather | bytes 540672 | tf_op jit(solution)/shard_map/all_gather | solution.py:301
  117.0 4.1 %collective-permute-start.1 = (bf16[2048,128]{1,0:T(8,128)(2,1)S(1)}, bf16[2048,128]{1,0:T(8,128)(2,1)S(1)}, u32[]{:S(2)}, u32[]{:S(2)}) collective-permute-start(bf16[2048,128]{1,0:T(8,128)(2,1)S(1)} %all_gather.26.mine), channel_id=1, source_target_pairs={{0,256},{256,0},{1,257},{257,1},{2,258},{258,2},{3,259},{259,3},{4... | collective-permute-start | bytes 1572872 | tf_op jit(solution)/shard_map/ppermute | solution.py:303
  121.1 0.1 pad_add_fusion.scal
  121.2 6.9 %collective-permute-done.1.theirs = bf16[2048,128]{1,0:T(8,128)(2,1)S(1)} collective-permute-done((bf16[2048,128]{1,0:T(8,128)(2,1)S(1)}, bf16[2048,128]{1,0:T(8,128)(2,1)S(1)}, u32[]{:S(2)}, u32[]{:S(2)}) %collective-permute-start.1) | collective-permute-done | bytes 524320 | tf_op jit(solution)/shard_map/ppermute | solution.py:303
  128.1 2.0 shard_map.101
  130.1 23.3 %all-gather.1 = bf16[3072,128]{1,0:T(8,128)(2,1)S(1)} all-gather(bf16[384,128]{1,0:T(8,128)(2,1)S(1)} %shard_map.101), channel_id=3, replica_groups=mesh['grp'=2,'fs'=32,'x'=4,'core'=2] {'x','core'}, dimensions={0}, use_global_device_ids=true | all-gather | bytes 884736 | tf_op jit(solution)/shard_map/all_gather | solution.py:312
  153.4 1.2 shard_map.102
  154.6 12.4 %all-gather.2 = bf16[1536,256]{1,0:T(8,128)(2,1)S(1)} all-gather(bf16[384,256]{1,0:T(8,128)(2,1)S(1)} %get-tuple-element.15), channel_id=4, replica_groups=mesh['grp'=2,'fs'=32,'x'=4,'core'=2] {'x'}, dimensions={0}, use_global_device_ids=true | all-gather | bytes 983040 | tf_op jit(solution)/shard_map/all_gather | solution.py:332
  167.0 3.5 %collective-permute-start.2 = (bf16[4,384,256]{2,1,0:T(8,128)(2,1)S(1)}, bf16[4,384,256]{2,1,0:T(8,128)(2,1)S(1)}, u32[]{:S(2)}, u32[]{:S(2)}) collective-permute-start(bf16[4,384,256]{2,1,0:T(8,128)(2,1)S(1)} %bitcast.20), channel_id=1, source_target_pairs={{0,1},{1,0},{2,3},{3,2},{4,5},{5,4},{6,7},{7,6},{8,9},{9,8},{10,11... | collective-permute-start | bytes 2359304 | tf_op jit(solution)/shard_map/ppermute | solution.py:246
  170.5 1.9 collective-permute-done.2.other
  172.4 1.1 shard_map.103
  173.5 1.1 copy-done
  174.6 0.7 copy-done.2
  175.3 11.5 %shard_map.104 = (bf16[3,384,256]{2,1,0:T(8,128)(2,1)}, bf16[4,384,256]{2,1,0:T(8,128)(2,1)}) custom-call(s32[3]{0:T(128)} %copy-done.4, bf16[384,2048]{1,0:T(8,128)(2,1)} %copy-done, f32[384,128]{1,0:T(8,128)} %copy-done.2, bf16[2048,2176]{1,0:T(8,128)(2,1)} %all-gather.5.cloned.1.call-done.weight), custom_call_target="tpu_custom_call" | custom-call | flops 2768240640 | bytes 5767168 | tf_op jit(solution)/shard_map/pallas_call | solution.py:349
  186.8 15.3 %collective-permute-start.3 = (bf16[4,384,256]{2,1,0:T(8,128)(2,1)}, bf16[4,384,256]{2,1,0:T(8,128)(2,1)S(1)}, u32[]{:S(2)}, u32[]{:S(2)}) collective-permute-start(bf16[4,384,256]{2,1,0:T(8,128)(2,1)} %get-tuple-element.20), channel_id=1, source_target_pairs={{0,1},{1,0},{2,3},{3,2},{4,5},{5,4},{6,7},{7,6},{8,9},{9,8},{10,11... | collective-permute-start | bytes 2359304 | tf_op jit(solution)/shard_map/ppermute | solution.py:246
  202.1 5.2 %shard_map.105 = f32[4,384,256]{2,1,0:T(8,128)} custom-call(s32[3]{0:T(128)} %copy-done.4, bf16[3,384,256]{2,1,0:T(8,128)(2,1)} %get-tuple-element.19.hidden, bf16[2048,2176]{1,0:T(8,128)(2,1)} %all-gather.5.cloned.1.call-done.weight), custom_call_target="tpu_custom_call" | custom-call | flops 553648128 | bytes 1441792 | tf_op jit(solution)/shard_map/pallas_call | solution.py:368
  207.3 1.6 add_convert_fusion
  208.9 16.1 %all_to_all.5 = bf16[4,384,256]{2,1,0:T(8,128)(2,1)S(1)} all-to-all(bf16[4,384,256]{2,1,0:T(8,128)(2,1)S(1)} %add_convert_fusion), channel_id=1, replica_groups=mesh['grp'=2,'fs'=32,'x'=4,'core'=2] {'x'}, dimensions={0} | all-to-all | bytes 1572864 | tf_op jit(solution)/shard_map/all_to_all | solution.py:378
  225.0 0.1 convert_reduce_fusion
  225.1 0.7 fusion
  (22 shorter events, 0.1 us)
Async XLA Ops:
  6.5 59.2 %copy-start.8 = (bf16[32,256]{1,0:T(8,128)(2,1)S(1)}, bf16[32,256]{1,0:T(8,128)(2,1)}, u32[]{:S(2)}) copy-start(bf16[32,256]{1,0:T(8,128)(2,1)} %param.15) | copy-start | bytes 49156
  6.5 59.2 %copy-start.7 = (bf16[64,128]{1,0:T(8,128)(2,1)S(1)}, bf16[64,128]{1,0:T(8,128)(2,1)}, u32[]{:S(2)}) copy-start(bf16[64,128]{1,0:T(8,128)(2,1)} %param.12) | copy-start | bytes 49156
  6.6 121.5 %copy-start.3 = (bf16[1,128,128]{2,1,0:T(8,128)(2,1)S(1)}, bf16[1,128,128]{2,1,0:T(8,128)(2,1)}, u32[]{:S(2)}) copy-start(bf16[1,128,128]{2,1,0:T(8,128)(2,1)} %pool_weight.1) | copy-start | bytes 98308
  6.6 121.5 %copy-start.6 = (f32[128]{0:T(128)S(1)}, f32[128]{0:T(128)}, u32[]{:S(2)}) copy-start(f32[128]{0:T(128)} %param.14) | copy-start | bytes 1540
  6.6 168.8 %all-gather.5.cloned.1.call-start = ((), (), s32[]{:S(2)}) async-start(), calls=%async_computation.1 | async-start | bytes 9191424 | tf_op jit(solution)/shard_map/all_gather | solution.py:293
  20.9 107.2 %collective-permute-start = (bf16[4,400,256]{2,1,0:T(8,128)(2,1)S(1)}, bf16[4,400,256]{2,1,0:T(8,128)(2,1)S(1)}, u32[]{:S(2)}, u32[]{:S(2)}) collective-permute-start(bf16[4,400,256]{2,1,0:T(8,128)(2,1)S(1)} %bitcast.15), channel_id=1, source_target_pairs={{0,1},{1,0},{2,3},{3,2},{4,5},{5,4},{6,7},{7,6},{8,9},{9,8},{10,11... | collective-permute-start | bytes 2457608 | tf_op jit(solution)/shard_map/ppermute | solution.py:246
  117.0 11.1 %collective-permute-start.1 = (bf16[2048,128]{1,0:T(8,128)(2,1)S(1)}, bf16[2048,128]{1,0:T(8,128)(2,1)S(1)}, u32[]{:S(2)}, u32[]{:S(2)}) collective-permute-start(bf16[2048,128]{1,0:T(8,128)(2,1)S(1)} %all_gather.26.mine), channel_id=1, source_target_pairs={{0,256},{256,0},{1,257},{257,1},{2,258},{258,2},{3,259},{259,3},{4... | collective-permute-start | bytes 1572872 | tf_op jit(solution)/shard_map/ppermute | solution.py:303
  121.2 51.2 %copy-start.4 = (s32[3]{0:T(128)}, s32[3]{0:T(128)S(1)}, u32[]{:S(2)}) copy-start(s32[3]{0:T(128)S(1)} %pad_add_fusion.scal) | copy-start | bytes 40
  128.1 25.3 %copy-start.1 = (bf16[1,384,256]{2,1,0:T(8,128)(2,1)S(1)}, bf16[1,384,256]{2,1,0:T(8,128)(2,1)}, u32[]{:S(2)}) copy-start(bf16[1,384,256]{2,1,0:T(8,128)(2,1)} %param.10) | copy-start | bytes 589828
  128.1 25.3 %copy-start.5 = (f32[256]{0:T(256)S(1)}, f32[256]{0:T(256)}, u32[]{:S(2)}) copy-start(f32[256]{0:T(256)} %param.16) | copy-start | bytes 3076
  167.0 5.4 %collective-permute-start.2 = (bf16[4,384,256]{2,1,0:T(8,128)(2,1)S(1)}, bf16[4,384,256]{2,1,0:T(8,128)(2,1)S(1)}, u32[]{:S(2)}, u32[]{:S(2)}) collective-permute-start(bf16[4,384,256]{2,1,0:T(8,128)(2,1)S(1)} %bitcast.20), channel_id=1, source_target_pairs={{0,1},{1,0},{2,3},{3,2},{4,5},{5,4},{6,7},{7,6},{8,9},{9,8},{10,11... | collective-permute-start | bytes 2359304 | tf_op jit(solution)/shard_map/ppermute | solution.py:246
  173.5 1.1 copy-start
  174.6 0.7 copy-start.2
  186.8 20.5 %collective-permute-start.3 = (bf16[4,384,256]{2,1,0:T(8,128)(2,1)}, bf16[4,384,256]{2,1,0:T(8,128)(2,1)S(1)}, u32[]{:S(2)}, u32[]{:S(2)}) collective-permute-start(bf16[4,384,256]{2,1,0:T(8,128)(2,1)} %get-tuple-element.20), channel_id=1, source_target_pairs={{0,1},{1,0},{2,3},{3,2},{4,5},{5,4},{6,7},{7,6},{8,9},{9,8},{10,11... | collective-permute-start | bytes 2359304 | tf_op jit(solution)/shard_map/ppermute | solution.py:246
Sparse Core Ops, SparseCore 0:
  9.5 161.6 all-gather.4

commit v3 on v2

--- a/solution.py
+++ b/solution.py
@@ -13,6 +13,7 @@
 LANES = 128
 EXTRA = 16
 VM = pltpu.VMEM
+HIDDEN_VMEM = 50
 F32, BF16 = jnp.float32, jnp.bfloat16
 
 
@@ -148,7 +149,7 @@
     scale[...] = jnp.broadcast_to(lax.rsqrt(square / D + EPSILON), scale.shape)
 
 
-def hidden_kernel(scal, features_at, scale, weight, hidden, partial, features, wide, down, sems, dsems):
+def hidden_kernel(scal, features_at, scale, weight, hidden, partial, kept, features, wide, down, sems, dsems):
     core = scal[0]
     chips, length, width = partial.shape
     blocks = wide.shape[0]
@@ -158,12 +159,12 @@
             weight.at[:, pl.ds(i * 2 * LANES, 2 * LANES)], wide.at[i], sems.at[i]
         )
 
-    def down_copy(chip):
-        row = pl.multiple_of((chip * CORES + 1 - core) * width, width)
+    def down_copy(chip, mine=False):
+        row = pl.multiple_of((chip * CORES + (core if mine else 1 - core)) * width, width)
         return pltpu.make_async_copy(
             weight.at[pl.ds(row, width), pl.ds(weight.shape[1] - down.shape[2], down.shape[2])],
-            down.at[chip],
-            dsems.at[chip],
+            (kept if mine else down).at[chip],
+            dsems.at[chips + chip if mine else chip],
         )
 
     feature_copy = pltpu.make_async_copy(features_at, features, sems.at[blocks])
@@ -172,6 +173,8 @@
         gate_copy(i).start()
     for chip in range(chips):
         down_copy(chip).start()
+    for chip in range(chips):
+        down_copy(chip, True).start()
     factor = scale[...]
     feature_copy.wait()
 
@@ -206,25 +209,13 @@
         for p in range(blocks // 2):
             total += dot_t(hidden[p], down[chip, :, p * 2 * LANES : (p + 1) * 2 * LANES])
         partial[chip] = total.astype(BF16)
-
-
-def down_kernel(scal, hidden, weight, partial, down, dsems):
-    core = scal[0]
-    chips, length, width = partial.shape
-
-    def down_copy(chip):
-        row = pl.multiple_of((chip * CORES + core) * width, width)
-        return pltpu.make_async_copy(
-            weight.at[pl.ds(row, width), pl.ds(weight.shape[1] - down.shape[2], down.shape[2])],
-            down.at[chip],
-            dsems.at[chip],
-        )
-
     for chip in range(chips):
-        down_copy(chip).start()
-    for chip in range(chips):
-        down_copy(chip).wait()
-        total = jnp.zeros((length, width), F32)
+        down_copy(chip, True).wait()
+
+
+def down_kernel(hidden, down, partial):
+    for chip in range(partial.shape[0]):
+        total = jnp.zeros(partial.shape[1:], F32)
         for p in range(hidden.shape[0]):
             total += dot_t(hidden[p], down[chip, :, p * 2 * LANES : (p + 1) * 2 * LANES])
         partial[chip] = total
@@ -342,27 +333,24 @@
         [smem] + [spec()] * 4,
     )(scal, own_two, other_two, own, other)
 
-    down_scratch = (
-        VM((chips, width, depth), BF16),
-        pltpu.SemaphoreType.DMA((chips,)),
-    )
-    hidden, partial_other = call(
+    hidden, partial_other, down_own = call(
         hidden_kernel,
         (
             jax.ShapeDtypeStruct((blocks // 2, length, 2 * LANES), BF16),
             jax.ShapeDtypeStruct((chips, length, width), BF16),
+            jax.ShapeDtypeStruct((chips, width, depth), BF16),
         ),
         5 * length * D * units,
-        4 * D * units,
+        6 * D * units,
         [smem, anywhere, spec(), anywhere],
         (
             VM(features.shape, BF16),
             VM((blocks, D, 2 * LANES), BF16),
-            down_scratch[0],
+            VM((chips, width, depth), BF16),
             pltpu.SemaphoreType.DMA((blocks + 1,)),
-            down_scratch[1],
-        ),
-        56,
+            pltpu.SemaphoreType.DMA((2 * chips,)),
+        ),
+        HIDDEN_VMEM,
     )(scal, features, scale_two, weight)
     arrived = swap(partial_other)
     partial_own = call(
@@ -370,10 +358,8 @@
         jax.ShapeDtypeStruct((chips, length, width), F32),
         length * D * units,
         D * units,
-        [smem, spec(), anywhere],
-        down_scratch,
-        56,
-    )(scal, hidden, weight)
+        [spec()] * 2,
+    )(hidden, down_own)
     paired = (partial_own + arrived.astype(F32)).astype(BF16)
     summed = lax.all_to_all(paired, "x", split_axis=0, concat_axis=0, tiled=True)
     return (mixed + summed.astype(F32).sum(axis=0)).astype(BF16)[None]

time: 233 us -> 227 us (0.974)
  Pallas kernels: 23 us -> 17.6 us
    pallas_call x1, Pallas kernels: 5.19 us -> 0.8 us  [local(): call(down_kernel, jax.ShapeDtypeStruct((chips, length, width), F32), leng...]
  transfers between devices with their start and end apart: 5 -> 5, of which waited for: 2 -> 3; matrix products, arithmetic and copies ran while one was open for 0% -> 0% of each run, Pallas kernels for 4% -> 2%
where the time goes in v3:
time: 227 us; the launch traced here: 226 us
  blocking collectives  115 us (51%)
  starting transfers between devices  68.5 us (30%)
  Pallas kernels  17.6 us (8%)
  between operations  13.6 us (6%)
  waiting for transfers between devices  9.63 us (4%)
    ppermute x3, starting transfers between devices, swap(): return lax.ppermute(array, 'core', [(0, 1), (1, 0)])  64.5 us
    all_gather x1, blocking collectives, local(): mine = lax.all_gather(chosen, 'fs', axis=0, tiled=True)  50.9 us
    all_gather x1, blocking collectives, local(): pooled_all = lax.all_gather(pooled, ('x', 'core'), axis=0)  23.9 us
    all_to_all x1, blocking collectives, local(): lax.all_to_all(paired, 'x', split_axis=0, concat_axis=0, tiled=True)  15.1 us
    all_gather x1, blocking collectives, local(): own_two = lax.all_gather(scaled, 'x', axis=0)  12.5 us
    all_gather x1, blocking collectives, local(): own = lax.all_gather(sent, 'x', axis=0)  12.2 us
    pallas_call x1, Pallas kernels, local(): call(hidden_kernel, (jax.ShapeDtypeStruct((blocks // 2, length, 2 * LANES...  10.5 us
    ppermute x1, waiting for transfers between devices, local(): theirs = lax.ppermute(mine, 'grp', [(i, i ^ 1) for i in range(groups)])  6.6 us
  transfers between devices with their start and end apart: 5, of which 3 were waited for; matrix products, arithmetic and copies ran while one was open for 0% of the time, Pallas kernels for 2%

profile of v3, /device:TPU:33, one launch (start us, length us, event | category | flops | bytes accessed | tf_op | source)
XLA Modules:
  0.0 226.3 jit_solution(1214638109102080853)
XLA Ops:
  6.6 0.1 all-gather.5.cloned.1.call-start
  6.6 2.0 shard_map.100
  8.7 12.2 %all-gather = bf16[1600,256]{1,0:T(8,128)(2,1)S(1)} all-gather(bf16[400,256]{1,0:T(8,128)(2,1)} %get-tuple-element.14), channel_id=2, replica_groups=mesh['grp'=2,'fs'=32,'x'=4,'core'=2] {'x'}, dimensions={0}, use_global_device_ids=true | all-gather | bytes 1024000 | tf_op jit(solution)/shard_map/all_gather | solution.py:286
  20.9 44.8 %collective-permute-start = (bf16[4,400,256]{2,1,0:T(8,128)(2,1)S(1)}, bf16[4,400,256]{2,1,0:T(8,128)(2,1)S(1)}, u32[]{:S(2)}, u32[]{:S(2)}) collective-permute-start(bf16[4,400,256]{2,1,0:T(8,128)(2,1)S(1)} %bitcast.15), channel_id=1, source_target_pairs={{0,1},{1,0},{2,3},{3,2},{4,5},{5,4},{6,7},{7,6},{8,9},{9,8},{10,11... | collective-permute-start | bytes 2457608 | tf_op jit(solution)/shard_map/ppermute | solution.py:237
  65.8 50.9 %all_gather.26.mine = bf16[2048,128]{1,0:T(8,128)(2,1)S(1)} all-gather(bf16[64,128]{1,0:T(8,128)(2,1)S(1)} %maximum_select_fusion), channel_id=1, replica_groups=mesh['grp'=2,'fs'=32,'x'=4,'core'=2] {'fs'}, dimensions={0}, use_global_device_ids=true | all-gather | bytes 540672 | tf_op jit(solution)/shard_map/all_gather | solution.py:292
  116.7 4.0 %collective-permute-start.1 = (bf16[2048,128]{1,0:T(8,128)(2,1)S(1)}, bf16[2048,128]{1,0:T(8,128)(2,1)S(1)}, u32[]{:S(2)}, u32[]{:S(2)}) collective-permute-start(bf16[2048,128]{1,0:T(8,128)(2,1)S(1)} %all_gather.26.mine), channel_id=1, source_target_pairs={{0,256},{256,0},{1,257},{257,1},{2,258},{258,2},{3,259},{259,3},{4... | collective-permute-start | bytes 1572872 | tf_op jit(solution)/shard_map/ppermute | solution.py:294
  120.7 0.1 pad_add_fusion.scal
  120.8 6.6 %collective-permute-done.1.theirs = bf16[2048,128]{1,0:T(8,128)(2,1)S(1)} collective-permute-done((bf16[2048,128]{1,0:T(8,128)(2,1)S(1)}, bf16[2048,128]{1,0:T(8,128)(2,1)S(1)}, u32[]{:S(2)}, u32[]{:S(2)}) %collective-permute-start.1) | collective-permute-done | bytes 524320 | tf_op jit(solution)/shard_map/ppermute | solution.py:294
  127.4 2.0 shard_map.101
  129.4 23.9 %all-gather.1 = bf16[3072,128]{1,0:T(8,128)(2,1)S(1)} all-gather(bf16[384,128]{1,0:T(8,128)(2,1)S(1)} %shard_map.101), channel_id=3, replica_groups=mesh['grp'=2,'fs'=32,'x'=4,'core'=2] {'x','core'}, dimensions={0}, use_global_device_ids=true | all-gather | bytes 884736 | tf_op jit(solution)/shard_map/all_gather | solution.py:303
  153.4 1.2 shard_map.102
  154.5 12.5 %all-gather.2 = bf16[1536,256]{1,0:T(8,128)(2,1)S(1)} all-gather(bf16[384,256]{1,0:T(8,128)(2,1)S(1)} %get-tuple-element.16), channel_id=4, replica_groups=mesh['grp'=2,'fs'=32,'x'=4,'core'=2] {'x'}, dimensions={0}, use_global_device_ids=true | all-gather | bytes 983040 | tf_op jit(solution)/shard_map/all_gather | solution.py:323
  167.0 3.4 %collective-permute-start.2 = (bf16[4,384,256]{2,1,0:T(8,128)(2,1)S(1)}, bf16[4,384,256]{2,1,0:T(8,128)(2,1)S(1)}, u32[]{:S(2)}, u32[]{:S(2)}) collective-permute-start(bf16[4,384,256]{2,1,0:T(8,128)(2,1)S(1)} %bitcast.20), channel_id=1, source_target_pairs={{0,1},{1,0},{2,3},{3,2},{4,5},{5,4},{6,7},{7,6},{8,9},{9,8},{10,11... | collective-permute-start | bytes 2359304 | tf_op jit(solution)/shard_map/ppermute | solution.py:237
  170.4 1.9 collective-permute-done.2.other
  172.3 1.1 shard_map.103
  173.4 1.1 copy-done
  174.6 10.5 %shard_map.104 = (bf16[3,384,256]{2,1,0:T(8,128)(2,1)S(1)}, bf16[4,384,256]{2,1,0:T(8,128)(2,1)S(1)}, bf16[4,256,768]{2,1,0:T(8,128)(2,1)S(1)}) custom-call(s32[3]{0:T(128)S(1)} %pad_add_fusion.scal, bf16[384,2048]{1,0:T(8,128)(2,1)} %copy-done, f32[384,128]{1,0:T(8,128)S(1)} %get-tuple-element.18.scale, bf16[2048,2176]{1,0:T(8,128)(2,1)} %all-gather.5.cloned.1.call-done.weight), custom_call_target="tpu_custom_call" | custom-call | flops 2768240640 | bytes 8650752 | tf_op jit(solution)/shard_map/pallas_call | solution.py:336
  185.1 16.2 %collective-permute-start.3 = (bf16[4,384,256]{2,1,0:T(8,128)(2,1)S(1)}, bf16[4,384,256]{2,1,0:T(8,128)(2,1)S(1)}, u32[]{:S(2)}, u32[]{:S(2)}) collective-permute-start(bf16[4,384,256]{2,1,0:T(8,128)(2,1)S(1)} %get-tuple-element.22), channel_id=1, source_target_pairs={{0,1},{1,0},{2,3},{3,2},{4,5},{5,4},{6,7},{7,6},{8,9},{9,8},{10,11... | collective-permute-start | bytes 2359304 | tf_op jit(solution)/shard_map/ppermute | solution.py:237
  201.3 0.8 shard_map.105
  202.1 1.1 collective-permute-done.3
  203.2 0.3 add_convert_fusion
  203.5 15.1 %all_to_all.5 = bf16[4,384,256]{2,1,0:T(8,128)(2,1)S(1)} all-to-all(bf16[4,384,256]{2,1,0:T(8,128)(2,1)S(1)} %add_convert_fusion), channel_id=1, replica_groups=mesh['grp'=2,'fs'=32,'x'=4,'core'=2] {'x'}, dimensions={0} | all-to-all | bytes 1572864 | tf_op jit(solution)/shard_map/all_to_all | solution.py:364
  218.6 0.1 convert_reduce_fusion
  218.7 0.7 fusion
  (18 shorter events, 0.1 us)
Async XLA Ops:
  6.5 59.2 %copy-start.6 = (bf16[32,256]{1,0:T(8,128)(2,1)S(1)}, bf16[32,256]{1,0:T(8,128)(2,1)}, u32[]{:S(2)}) copy-start(bf16[32,256]{1,0:T(8,128)(2,1)} %param.15) | copy-start | bytes 49156
  6.5 59.2 %copy-start.5 = (bf16[64,128]{1,0:T(8,128)(2,1)S(1)}, bf16[64,128]{1,0:T(8,128)(2,1)}, u32[]{:S(2)}) copy-start(bf16[64,128]{1,0:T(8,128)(2,1)} %param.12) | copy-start | bytes 49156
  6.6 120.8 %copy-start.2 = (bf16[1,128,128]{2,1,0:T(8,128)(2,1)S(1)}, bf16[1,128,128]{2,1,0:T(8,128)(2,1)}, u32[]{:S(2)}) copy-start(bf16[1,128,128]{2,1,0:T(8,128)(2,1)} %pool_weight.1) | copy-start | bytes 98308
  6.6 120.8 %copy-start.4 = (f32[128]{0:T(128)S(1)}, f32[128]{0:T(128)}, u32[]{:S(2)}) copy-start(f32[128]{0:T(128)} %param.14) | copy-start | bytes 1540
  6.6 168.0 %all-gather.5.cloned.1.call-start = ((), (), s32[]{:S(2)}) async-start(), calls=%async_computation.1 | async-start | bytes 9191424 | tf_op jit(solution)/shard_map/all_gather | solution.py:284
  20.9 106.5 %collective-permute-start = (bf16[4,400,256]{2,1,0:T(8,128)(2,1)S(1)}, bf16[4,400,256]{2,1,0:T(8,128)(2,1)S(1)}, u32[]{:S(2)}, u32[]{:S(2)}) collective-permute-start(bf16[4,400,256]{2,1,0:T(8,128)(2,1)S(1)} %bitcast.15), channel_id=1, source_target_pairs={{0,1},{1,0},{2,3},{3,2},{4,5},{5,4},{6,7},{7,6},{8,9},{9,8},{10,11... | collective-permute-start | bytes 2457608 | tf_op jit(solution)/shard_map/ppermute | solution.py:237
  116.7 10.7 %collective-permute-start.1 = (bf16[2048,128]{1,0:T(8,128)(2,1)S(1)}, bf16[2048,128]{1,0:T(8,128)(2,1)S(1)}, u32[]{:S(2)}, u32[]{:S(2)}) collective-permute-start(bf16[2048,128]{1,0:T(8,128)(2,1)S(1)} %all_gather.26.mine), channel_id=1, source_target_pairs={{0,256},{256,0},{1,257},{257,1},{2,258},{258,2},{3,259},{259,3},{4... | collective-permute-start | bytes 1572872 | tf_op jit(solution)/shard_map/ppermute | solution.py:294
  127.4 25.9 %copy-start.1 = (bf16[1,384,256]{2,1,0:T(8,128)(2,1)S(1)}, bf16[1,384,256]{2,1,0:T(8,128)(2,1)}, u32[]{:S(2)}) copy-start(bf16[1,384,256]{2,1,0:T(8,128)(2,1)} %param.10) | copy-start | bytes 589828
  127.4 25.9 %copy-start.3 = (f32[256]{0:T(256)S(1)}, f32[256]{0:T(256)}, u32[]{:S(2)}) copy-start(f32[256]{0:T(256)} %param.16) | copy-start | bytes 3076
  167.0 5.3 %collective-permute-start.2 = (bf16[4,384,256]{2,1,0:T(8,128)(2,1)S(1)}, bf16[4,384,256]{2,1,0:T(8,128)(2,1)S(1)}, u32[]{:S(2)}, u32[]{:S(2)}) collective-permute-start(bf16[4,384,256]{2,1,0:T(8,128)(2,1)S(1)} %bitcast.20), channel_id=1, source_target_pairs={{0,1},{1,0},{2,3},{3,2},{4,5},{5,4},{6,7},{7,6},{8,9},{9,8},{10,11... | collective-permute-start | bytes 2359304 | tf_op jit(solution)/shard_map/ppermute | solution.py:237
  173.4 1.2 copy-start
  185.1 18.1 %collective-permute-start.3 = (bf16[4,384,256]{2,1,0:T(8,128)(2,1)S(1)}, bf16[4,384,256]{2,1,0:T(8,128)(2,1)S(1)}, u32[]{:S(2)}, u32[]{:S(2)}) collective-permute-start(bf16[4,384,256]{2,1,0:T(8,128)(2,1)S(1)} %get-tuple-element.22), channel_id=1, source_target_pairs={{0,1},{1,0},{2,3},{3,2},{4,5},{5,4},{6,7},{7,6},{8,9},{9,8},{10,11... | collective-permute-start | bytes 2359304 | tf_op jit(solution)/shard_map/ppermute | solution.py:237
Sparse Core Ops, SparseCore 0:
  9.5 162.2 all-gather.4

commit v4 on v3

--- a/solution.py
+++ b/solution.py
@@ -142,75 +142,70 @@
         for chip in range(chips):
             gain = gain_row(gains[chip, length:, :], 3)
             block = side[chip]
-            column = pl.multiple_of((chip * CORES + which) * width, width)
-            features[:, pl.ds(column, width)] = block
+            features[chip, :, pl.ds(pl.multiple_of(which * width, width), width)] = block
             part = block.astype(F32)
             square += jnp.sum(part * part * (1.0 / (gain * gain)), axis=1, keepdims=True)
     scale[...] = jnp.broadcast_to(lax.rsqrt(square / D + EPSILON), scale.shape)
 
 
-def hidden_kernel(scal, features_at, scale, weight, hidden, partial, kept, features, wide, down, sems, dsems):
+def hidden_kernel(
+    scal, features_at, scale, weight, hidden, partial, kept, features, wide, total, sems
+):
     core = scal[0]
     chips, length, width = partial.shape
-    blocks = wide.shape[0]
-
-    def gate_copy(i):
+    bands, depth, _ = wide.shape
+    gated = total.shape[1]
+
+    def band_copy(band):
+        row = pl.multiple_of(band * depth, depth)
         return pltpu.make_async_copy(
-            weight.at[:, pl.ds(i * 2 * LANES, 2 * LANES)], wide.at[i], sems.at[i]
+            weight.at[pl.ds(row, depth), :], wide.at[band], sems.at[band]
         )
 
-    def down_copy(chip, mine=False):
-        row = pl.multiple_of((chip * CORES + (core if mine else 1 - core)) * width, width)
-        return pltpu.make_async_copy(
-            weight.at[pl.ds(row, width), pl.ds(weight.shape[1] - down.shape[2], down.shape[2])],
-            (kept if mine else down).at[chip],
-            dsems.at[chips + chip if mine else chip],
-        )
-
-    feature_copy = pltpu.make_async_copy(features_at, features, sems.at[blocks])
+    feature_copy = pltpu.make_async_copy(features_at, features, sems.at[bands])
     feature_copy.start()
-    for i in range(blocks):
-        gate_copy(i).start()
-    for chip in range(chips):
-        down_copy(chip).start()
-    for chip in range(chips):
-        down_copy(chip, True).start()
+    for band in range(bands):
+        band_copy(band).start()
     factor = scale[...]
     feature_copy.wait()
-
-    def product(i, columns):
-        return dot(features[...], wide[i, :, :columns])
+    steps = [(at, min(2 * LANES, gated - at)) for at in range(0, gated, 2 * LANES)]
+
+    def add_band(band, first):
+        band_copy(band).wait()
+        for at, size in steps:
+            part = dot(features[band], wide[band, :, at : at + size])
+            total[:, at : at + size] = part if first else total[:, at : at + size] + part
+
+    add_band(0, True)
+
+    def later(band, carry):
+        add_band(band, False)
+        return carry
+
+    lax.fori_loop(1, bands, later, 0)
 
     def activated(gate, up):
         return (gate / (1.0 + jnp.exp(-gate))) * up
 
-    def full_block(i):
-        both = product(i, 2 * LANES)
-        return activated(both[:, :LANES] * factor, both[:, LANES:] * factor).astype(BF16)
-
-    def pair(p, carry):
-        for j in range(2):
-            gate_copy(2 * p + j).wait()
-            hidden[p, :, j * LANES : (j + 1) * LANES] = full_block(2 * p + j)
-        return carry
-
-    lax.fori_loop(0, blocks // 2 - 1, pair, 0)
-    last = blocks // 2 - 1
-    gate_copy(blocks - 2).wait()
-    hidden[last, :, :LANES] = full_block(blocks - 2)
-    gate_copy(blocks - 1).wait()
-    both = product(blocks - 1, LANES) * factor
-    lane = lax.broadcasted_iota(jnp.int32, both.shape, 1)
-    turned = pltpu.roll(both, LANES // 2, 1)
-    hidden[last, :, LANES:] = jnp.where(lane < LANES // 2, activated(both, turned), 0.0).astype(BF16)
+    for i, (at, size) in enumerate(steps):
+        pair, side = divmod(i, 2)
+        if size == 2 * LANES:
+            gate = total[:, at : at + LANES] * factor
+            value = activated(gate, total[:, at + LANES : at + size] * factor)
+        else:
+            both = total[:, at : at + size] * factor
+            lane = lax.broadcasted_iota(jnp.int32, both.shape, 1)
+            turned = pltpu.roll(both, LANES // 2, 1)
+            value = jnp.where(lane < LANES // 2, activated(both, turned), 0.0)
+        hidden[pair, :, side * LANES : (side + 1) * LANES] = value.astype(BF16)
     for chip in range(chips):
-        down_copy(chip).wait()
-        total = jnp.zeros((length, width), F32)
-        for p in range(blocks // 2):
-            total += dot_t(hidden[p], down[chip, :, p * 2 * LANES : (p + 1) * 2 * LANES])
-        partial[chip] = total.astype(BF16)
-    for chip in range(chips):
-        down_copy(chip, True).wait()
+        theirs = pl.multiple_of((1 - core) * width, width)
+        product = jnp.zeros((length, width), F32)
+        for p in range(hidden.shape[0]):
+            at = gated + p * 2 * LANES
+            product += dot_t(hidden[p], wide[chip, pl.ds(theirs, width), at : at + 2 * LANES])
+        partial[chip] = product.astype(BF16)
+        kept[chip] = wide[chip, pl.ds(pl.multiple_of(core * width, width), width), gated:]
 
 
 def down_kernel(hidden, down, partial):
@@ -326,7 +321,7 @@
         square_kernel,
         (
             jax.ShapeDtypeStruct((length, LANES), F32),
-            jax.ShapeDtypeStruct((length, chips * CORES * width), BF16),
+            jax.ShapeDtypeStruct((chips, length, CORES * width), BF16),
         ),
         6 * length * D,
         4 * length * D,
@@ -345,10 +340,9 @@
         [smem, anywhere, spec(), anywhere],
         (
             VM(features.shape, BF16),
-            VM((blocks, D, 2 * LANES), BF16),
-            VM((chips, width, depth), BF16),
-            pltpu.SemaphoreType.DMA((blocks + 1,)),
-            pltpu.SemaphoreType.DMA((2 * chips,)),
+            VM((chips, CORES * width, weight.shape[1]), BF16),
+            VM((length, 2 * units), F32),
+            pltpu.SemaphoreType.DMA((chips + 1,)),
         ),
         HIDDEN_VMEM,
     )(scal, features, scale_two, weight)

time: 227 us -> 223 us (0.982)
  Pallas kernels: 17.6 us -> 13.9 us
    pallas_call x1, Pallas kernels: 10.5 us -> 6.81 us  [local(): call(hidden_kernel, (jax.ShapeDtypeStruct((blocks // 2, length, 2 * LANES...]
where the time goes in v4:
time: 223 us
  blocking collectives  115 us (52%)
  starting transfers between devices  68.5 us (31%)
  Pallas kernels  13.9 us (6%)
  between operations  13.6 us (6%)
  waiting for transfers between devices  9.63 us (4%)
    ppermute x3, starting transfers between devices, swap(): return lax.ppermute(array, 'core', [(0, 1), (1, 0)])  64.5 us
    all_gather x1, blocking collectives, local(): mine = lax.all_gather(chosen, 'fs', axis=0, tiled=True)  50.9 us
    all_gather x1, blocking collectives, local(): pooled_all = lax.all_gather(pooled, ('x', 'core'), axis=0)  23.9 us
    all_to_all x1, blocking collectives, local(): lax.all_to_all(paired, 'x', split_axis=0, concat_axis=0, tiled=True)  15.1 us
    all_gather x1, blocking collectives, local(): own_two = lax.all_gather(scaled, 'x', axis=0)  12.5 us
    all_gather x1, blocking collectives, local(): own = lax.all_gather(sent, 'x', axis=0)  12.2 us
    pallas_call x1, Pallas kernels, local(): call(hidden_kernel, (jax.ShapeDtypeStruct((blocks // 2, length, 2 * LANES...  6.81 us
    ppermute x1, waiting for transfers between devices, local(): theirs = lax.ppermute(mine, 'grp', [(i, i ^ 1) for i in range(groups)])  6.6 us
  transfers between devices with their start and end apart: 5, of which 3 were waited for; matrix products, arithmetic and copies ran while one was open for 0% of the time, Pallas kernels for 2%

profile of v4, /device:TPU:33, one launch (start us, length us, event | category | flops | bytes accessed | tf_op | source)
XLA Modules:
  0.0 222.6 jit_solution(3666002919794033237)
XLA Ops:
  6.6 0.1 all-gather.5.cloned.1.call-start
  6.6 2.0 shard_map.100
  8.7 12.2 %all-gather = bf16[1600,256]{1,0:T(8,128)(2,1)S(1)} all-gather(bf16[400,256]{1,0:T(8,128)(2,1)} %get-tuple-element.14), channel_id=2, replica_groups=mesh['grp'=2,'fs'=32,'x'=4,'core'=2] {'x'}, dimensions={0}, use_global_device_ids=true | all-gather | bytes 1024000 | tf_op jit(solution)/shard_map/all_gather | solution.py:281
  20.9 44.8 %collective-permute-start = (bf16[4,400,256]{2,1,0:T(8,128)(2,1)S(1)}, bf16[4,400,256]{2,1,0:T(8,128)(2,1)S(1)}, u32[]{:S(2)}, u32[]{:S(2)}) collective-permute-start(bf16[4,400,256]{2,1,0:T(8,128)(2,1)S(1)} %bitcast.15), channel_id=1, source_target_pairs={{0,1},{1,0},{2,3},{3,2},{4,5},{5,4},{6,7},{7,6},{8,9},{9,8},{10,11... | collective-permute-start | bytes 2457608 | tf_op jit(solution)/shard_map/ppermute | solution.py:232
  65.8 50.9 %all_gather.26.mine = bf16[2048,128]{1,0:T(8,128)(2,1)S(1)} all-gather(bf16[64,128]{1,0:T(8,128)(2,1)S(1)} %maximum_select_fusion), channel_id=1, replica_groups=mesh['grp'=2,'fs'=32,'x'=4,'core'=2] {'fs'}, dimensions={0}, use_global_device_ids=true | all-gather | bytes 540672 | tf_op jit(solution)/shard_map/all_gather | solution.py:287
  116.7 4.0 %collective-permute-start.1 = (bf16[2048,128]{1,0:T(8,128)(2,1)S(1)}, bf16[2048,128]{1,0:T(8,128)(2,1)S(1)}, u32[]{:S(2)}, u32[]{:S(2)}) collective-permute-start(bf16[2048,128]{1,0:T(8,128)(2,1)S(1)} %all_gather.26.mine), channel_id=1, source_target_pairs={{0,256},{256,0},{1,257},{257,1},{2,258},{258,2},{3,259},{259,3},{4... | collective-permute-start | bytes 1572872 | tf_op jit(solution)/shard_map/ppermute | solution.py:289
  120.7 0.1 pad_add_fusion.scal
  120.8 6.6 %collective-permute-done.1.theirs = bf16[2048,128]{1,0:T(8,128)(2,1)S(1)} collective-permute-done((bf16[2048,128]{1,0:T(8,128)(2,1)S(1)}, bf16[2048,128]{1,0:T(8,128)(2,1)S(1)}, u32[]{:S(2)}, u32[]{:S(2)}) %collective-permute-start.1) | collective-permute-done | bytes 524320 | tf_op jit(solution)/shard_map/ppermute | solution.py:289
  127.4 2.0 shard_map.101
  129.4 23.9 %all-gather.1 = bf16[3072,128]{1,0:T(8,128)(2,1)S(1)} all-gather(bf16[384,128]{1,0:T(8,128)(2,1)S(1)} %shard_map.101), channel_id=3, replica_groups=mesh['grp'=2,'fs'=32,'x'=4,'core'=2] {'x','core'}, dimensions={0}, use_global_device_ids=true | all-gather | bytes 884736 | tf_op jit(solution)/shard_map/all_gather | solution.py:298
  153.4 1.2 shard_map.102
  154.5 12.5 %all-gather.2 = bf16[1536,256]{1,0:T(8,128)(2,1)S(1)} all-gather(bf16[384,256]{1,0:T(8,128)(2,1)S(1)} %get-tuple-element.16), channel_id=4, replica_groups=mesh['grp'=2,'fs'=32,'x'=4,'core'=2] {'x'}, dimensions={0}, use_global_device_ids=true | all-gather | bytes 983040 | tf_op jit(solution)/shard_map/all_gather | solution.py:318
  167.0 3.4 %collective-permute-start.2 = (bf16[4,384,256]{2,1,0:T(8,128)(2,1)S(1)}, bf16[4,384,256]{2,1,0:T(8,128)(2,1)S(1)}, u32[]{:S(2)}, u32[]{:S(2)}) collective-permute-start(bf16[4,384,256]{2,1,0:T(8,128)(2,1)S(1)} %bitcast.20), channel_id=1, source_target_pairs={{0,1},{1,0},{2,3},{3,2},{4,5},{5,4},{6,7},{7,6},{8,9},{9,8},{10,11... | collective-permute-start | bytes 2359304 | tf_op jit(solution)/shard_map/ppermute | solution.py:232
  170.4 1.9 collective-permute-done.2.other
  172.3 1.1 shard_map.103
  173.4 1.1 copy-done
  174.6 6.8 %shard_map.104 = (bf16[3,384,256]{2,1,0:T(8,128)(2,1)S(1)}, bf16[4,384,256]{2,1,0:T(8,128)(2,1)S(1)}, bf16[4,256,768]{2,1,0:T(8,128)(2,1)S(1)}) custom-call(s32[3]{0:T(128)S(1)} %pad_add_fusion.scal, bf16[4,384,512]{2,1,0:T(8,128)(2,1)} %copy-done, f32[384,128]{1,0:T(8,128)S(1)} %get-tuple-element.18.scale, ...), custom_call_target="tpu_custom_call" | custom-call | flops 2768240640 | bytes 8650752 | tf_op jit(solution)/shard_map/pallas_call | solution.py:331
  181.4 16.2 %collective-permute-start.3 = (bf16[4,384,256]{2,1,0:T(8,128)(2,1)S(1)}, bf16[4,384,256]{2,1,0:T(8,128)(2,1)S(1)}, u32[]{:S(2)}, u32[]{:S(2)}) collective-permute-start(bf16[4,384,256]{2,1,0:T(8,128)(2,1)S(1)} %get-tuple-element.22), channel_id=1, source_target_pairs={{0,1},{1,0},{2,3},{3,2},{4,5},{5,4},{6,7},{7,6},{8,9},{9,8},{10,11... | collective-permute-start | bytes 2359304 | tf_op jit(solution)/shard_map/ppermute | solution.py:232
  197.6 0.8 shard_map.105
  198.4 1.1 collective-permute-done.3
  199.5 0.3 add_convert_fusion
  199.8 15.1 %all_to_all.5 = bf16[4,384,256]{2,1,0:T(8,128)(2,1)S(1)} all-to-all(bf16[4,384,256]{2,1,0:T(8,128)(2,1)S(1)} %add_convert_fusion), channel_id=1, replica_groups=mesh['grp'=2,'fs'=32,'x'=4,'core'=2] {'x'}, dimensions={0} | all-to-all | bytes 1572864 | tf_op jit(solution)/shard_map/all_to_all | solution.py:358
  214.9 0.1 convert_reduce_fusion
  215.0 0.7 fusion
  (18 shorter events, 0.1 us)
Async XLA Ops:
  6.5 59.2 %copy-start.6 = (bf16[32,256]{1,0:T(8,128)(2,1)S(1)}, bf16[32,256]{1,0:T(8,128)(2,1)}, u32[]{:S(2)}) copy-start(bf16[32,256]{1,0:T(8,128)(2,1)} %param.15) | copy-start | bytes 49156
  6.5 59.2 %copy-start.5 = (bf16[64,128]{1,0:T(8,128)(2,1)S(1)}, bf16[64,128]{1,0:T(8,128)(2,1)}, u32[]{:S(2)}) copy-start(bf16[64,128]{1,0:T(8,128)(2,1)} %param.12) | copy-start | bytes 49156
  6.6 120.8 %copy-start.2 = (bf16[1,128,128]{2,1,0:T(8,128)(2,1)S(1)}, bf16[1,128,128]{2,1,0:T(8,128)(2,1)}, u32[]{:S(2)}) copy-start(bf16[1,128,128]{2,1,0:T(8,128)(2,1)} %pool_weight.1) | copy-start | bytes 98308
  6.6 120.8 %copy-start.4 = (f32[128]{0:T(128)S(1)}, f32[128]{0:T(128)}, u32[]{:S(2)}) copy-start(f32[128]{0:T(128)} %param.14) | copy-start | bytes 1540
  6.6 168.0 %all-gather.5.cloned.1.call-start = ((), (), s32[]{:S(2)}) async-start(), calls=%async_computation.1 | async-start | bytes 9191424 | tf_op jit(solution)/shard_map/all_gather | solution.py:279
  20.9 106.5 %collective-permute-start = (bf16[4,400,256]{2,1,0:T(8,128)(2,1)S(1)}, bf16[4,400,256]{2,1,0:T(8,128)(2,1)S(1)}, u32[]{:S(2)}, u32[]{:S(2)}) collective-permute-start(bf16[4,400,256]{2,1,0:T(8,128)(2,1)S(1)} %bitcast.15), channel_id=1, source_target_pairs={{0,1},{1,0},{2,3},{3,2},{4,5},{5,4},{6,7},{7,6},{8,9},{9,8},{10,11... | collective-permute-start | bytes 2457608 | tf_op jit(solution)/shard_map/ppermute | solution.py:232
  116.7 10.7 %collective-permute-start.1 = (bf16[2048,128]{1,0:T(8,128)(2,1)S(1)}, bf16[2048,128]{1,0:T(8,128)(2,1)S(1)}, u32[]{:S(2)}, u32[]{:S(2)}) collective-permute-start(bf16[2048,128]{1,0:T(8,128)(2,1)S(1)} %all_gather.26.mine), channel_id=1, source_target_pairs={{0,256},{256,0},{1,257},{257,1},{2,258},{258,2},{3,259},{259,3},{4... | collective-permute-start | bytes 1572872 | tf_op jit(solution)/shard_map/ppermute | solution.py:289
  127.4 25.9 %copy-start.1 = (bf16[1,384,256]{2,1,0:T(8,128)(2,1)S(1)}, bf16[1,384,256]{2,1,0:T(8,128)(2,1)}, u32[]{:S(2)}) copy-start(bf16[1,384,256]{2,1,0:T(8,128)(2,1)} %param.10) | copy-start | bytes 589828
  127.4 25.9 %copy-start.3 = (f32[256]{0:T(256)S(1)}, f32[256]{0:T(256)}, u32[]{:S(2)}) copy-start(f32[256]{0:T(256)} %param.16) | copy-start | bytes 3076
  167.0 5.3 %collective-permute-start.2 = (bf16[4,384,256]{2,1,0:T(8,128)(2,1)S(1)}, bf16[4,384,256]{2,1,0:T(8,128)(2,1)S(1)}, u32[]{:S(2)}, u32[]{:S(2)}) collective-permute-start(bf16[4,384,256]{2,1,0:T(8,128)(2,1)S(1)} %bitcast.20), channel_id=1, source_target_pairs={{0,1},{1,0},{2,3},{3,2},{4,5},{5,4},{6,7},{7,6},{8,9},{9,8},{10,11... | collective-permute-start | bytes 2359304 | tf_op jit(solution)/shard_map/ppermute | solution.py:232
  173.4 1.2 copy-start
  181.4 18.1 %collective-permute-start.3 = (bf16[4,384,256]{2,1,0:T(8,128)(2,1)S(1)}, bf16[4,384,256]{2,1,0:T(8,128)(2,1)S(1)}, u32[]{:S(2)}, u32[]{:S(2)}) collective-permute-start(bf16[4,384,256]{2,1,0:T(8,128)(2,1)S(1)} %get-tuple-element.22), channel_id=1, source_target_pairs={{0,1},{1,0},{2,3},{3,2},{4,5},{5,4},{6,7},{7,6},{8,9},{9,8},{10,11... | collective-permute-start | bytes 2359304 | tf_op jit(solution)/shard_map/ppermute | solution.py:232
Sparse Core Ops, SparseCore 0:
  9.5 162.2 all-gather.4

commit v5 on v4

--- a/solution.py
+++ b/solution.py
@@ -276,7 +276,17 @@
         [VM(a.shape, a.dtype) for a in unpacked] + [pltpu.SemaphoreType.DMA((6,))],
         63,
     )(*unpacked)
-    weight = lax.all_gather(packed, "fs", axis=0, tiled=True)
+    length_fs = lax.axis_size("fs")
+    place = [(z * CORES + c, z * CORES + (c + z) % CORES) for z in range(length_fs) for c in range(CORES)]
+    packed = lax.ppermute(packed, ("fs", "core"), place)
+    rings = [
+        [(z * chips + x) * CORES + (c + z) % CORES for z in range(length_fs)]
+        for x in range(chips)
+        for c in range(CORES)
+    ]
+    weight = lax.all_gather(
+        packed, ("fs", "x", "core"), axis=0, tiled=True, axis_index_groups=rings
+    )
 
     own = lax.all_gather(sent, "x", axis=0)
     other = swap(own)

time: 223 us -> 217 us (0.973)
  starting transfers between devices: 68.5 us -> 56.7 us
  blocking collectives: 115 us -> 118 us
  waiting for transfers between devices: 9.63 us -> 12.1 us
    ppermute x3, starting transfers between devices: 64.5 us -> 51.4 us  [swap(): return lax.ppermute(array, 'core', [(0, 1), (1, 0)])]
    all_gather x1, blocking collectives: 50.9 us -> 53.8 us  [local(): mine = lax.all_gather(chosen, 'fs', axis=0, tiled=True)]
  transfers between devices with their start and end apart: 5 -> 6, of which waited for: 3 -> 4; matrix products, arithmetic and copies ran while one was open for 0% -> 0% of each run, Pallas kernels for 2% -> 2%
where the time goes in v5:
time: 217 us
  blocking collectives  118 us (54%)
  starting transfers between devices  56.7 us (26%)
  Pallas kernels  13.9 us (6%)
  between operations  13.6 us (6%)
  waiting for transfers between devices  12.1 us (6%)
    all_gather x1, blocking collectives, local(): mine = lax.all_gather(chosen, 'fs', axis=0, tiled=True)  53.8 us
    ppermute x3, starting transfers between devices, swap(): return lax.ppermute(array, 'core', [(0, 1), (1, 0)])  51.4 us
    all_gather x1, blocking collectives, local(): pooled_all = lax.all_gather(pooled, ('x', 'core'), axis=0)  24 us
    all_to_all x1, blocking collectives, local(): lax.all_to_all(paired, 'x', split_axis=0, concat_axis=0, tiled=True)  15.4 us
    all_gather x1, blocking collectives, local(): own = lax.all_gather(sent, 'x', axis=0)  12.2 us
    all_gather x1, blocking collectives, local(): own_two = lax.all_gather(scaled, 'x', axis=0)  12.2 us
    ppermute x1, waiting for transfers between devices, local(): theirs = lax.ppermute(mine, 'grp', [(i, i ^ 1) for i in range(groups)])  6.86 us
    pallas_call x1, Pallas kernels, local(): call(hidden_kernel, (jax.ShapeDtypeStruct((blocks // 2, length, 2 * LANES...  6.81 us
  transfers between devices with their start and end apart: 6, of which 4 were waited for; matrix products, arithmetic and copies ran while one was open for 0% of the time, Pallas kernels for 2%

profile of v5, /device:TPU:33, one launch (start us, length us, event | category | flops | bytes accessed | tf_op | source)
XLA Modules:
  0.0 216.9 jit_solution(9986356427949956491)
XLA Ops:
  6.6 2.1 shard_map.100
  8.7 1.6 collective-permute-start.3
  10.3 0.7 copy-done.5
  11.1 12.2 %all-gather = bf16[1600,256]{1,0:T(8,128)(2,1)S(1)} all-gather(bf16[400,256]{1,0:T(8,128)(2,1)} %get-tuple-element.14), channel_id=2, replica_groups=mesh['grp'=2,'fs'=32,'x'=4,'core'=2] {'x'}, dimensions={0}, use_global_device_ids=true | all-gather | bytes 1024000 | tf_op jit(solution)/shard_map/all_gather | solution.py:291
  23.3 44.8 %collective-permute-start = (bf16[4,400,256]{2,1,0:T(8,128)(2,1)S(1)}, bf16[4,400,256]{2,1,0:T(8,128)(2,1)S(1)}, u32[]{:S(2)}, u32[]{:S(2)}) collective-permute-start(bf16[4,400,256]{2,1,0:T(8,128)(2,1)S(1)} %bitcast.15), channel_id=1, source_target_pairs={{0,1},{1,0},{2,3},{3,2},{4,5},{5,4},{6,7},{7,6},{8,9},{9,8},{10,11... | collective-permute-start | bytes 2457608 | tf_op jit(solution)/shard_map/ppermute | solution.py:232
  68.1 53.8 %all_gather.26.mine = bf16[2048,128]{1,0:T(8,128)(2,1)S(1)} all-gather(bf16[64,128]{1,0:T(8,128)(2,1)S(1)} %maximum_select_fusion), channel_id=1, replica_groups=mesh['grp'=2,'fs'=32,'x'=4,'core'=2] {'fs'}, dimensions={0}, use_global_device_ids=true | all-gather | bytes 540672 | tf_op jit(solution)/shard_map/all_gather | solution.py:297
  121.9 3.7 %collective-permute-start.1 = (bf16[2048,128]{1,0:T(8,128)(2,1)S(1)}, bf16[2048,128]{1,0:T(8,128)(2,1)S(1)}, u32[]{:S(2)}, u32[]{:S(2)}) collective-permute-start(bf16[2048,128]{1,0:T(8,128)(2,1)S(1)} %all_gather.26.mine), channel_id=1, source_target_pairs={{0,256},{256,0},{1,257},{257,1},{2,258},{258,2},{3,259},{259,3},{4... | collective-permute-start | bytes 1572872 | tf_op jit(solution)/shard_map/ppermute | solution.py:299
  125.7 6.9 %collective-permute-done.1.theirs = bf16[2048,128]{1,0:T(8,128)(2,1)S(1)} collective-permute-done((bf16[2048,128]{1,0:T(8,128)(2,1)S(1)}, bf16[2048,128]{1,0:T(8,128)(2,1)S(1)}, u32[]{:S(2)}, u32[]{:S(2)}) %collective-permute-start.1) | collective-permute-done | bytes 524320 | tf_op jit(solution)/shard_map/ppermute | solution.py:299
  132.6 2.0 shard_map.101
  134.6 24.0 %all-gather.1 = bf16[3072,128]{1,0:T(8,128)(2,1)S(1)} all-gather(bf16[384,128]{1,0:T(8,128)(2,1)S(1)} %shard_map.101), channel_id=3, replica_groups=mesh['grp'=2,'fs'=32,'x'=4,'core'=2] {'x','core'}, dimensions={0}, use_global_device_ids=true | all-gather | bytes 884736 | tf_op jit(solution)/shard_map/all_gather | solution.py:308
  158.7 1.2 shard_map.102
  159.8 12.2 %all-gather.2 = bf16[1536,256]{1,0:T(8,128)(2,1)S(1)} all-gather(bf16[384,256]{1,0:T(8,128)(2,1)S(1)} %get-tuple-element.16), channel_id=4, replica_groups=mesh['grp'=2,'fs'=32,'x'=4,'core'=2] {'x'}, dimensions={0}, use_global_device_ids=true | all-gather | bytes 983040 | tf_op jit(solution)/shard_map/all_gather | solution.py:328
  172.0 3.7 %collective-permute-start.2 = (bf16[4,384,256]{2,1,0:T(8,128)(2,1)S(1)}, bf16[4,384,256]{2,1,0:T(8,128)(2,1)S(1)}, u32[]{:S(2)}, u32[]{:S(2)}) collective-permute-start(bf16[4,384,256]{2,1,0:T(8,128)(2,1)S(1)} %bitcast.20), channel_id=1, source_target_pairs={{0,1},{1,0},{2,3},{3,2},{4,5},{5,4},{6,7},{7,6},{8,9},{9,8},{10,11... | collective-permute-start | bytes 2359304 | tf_op jit(solution)/shard_map/ppermute | solution.py:232
  175.7 1.9 collective-permute-done.2.other
  177.6 1.1 shard_map.103
  178.7 1.1 copy-done
  179.9 2.2 %all-gather.5.cloned.1.call-done.weight = bf16[2048,2176]{1,0:T(8,128)(2,1)} async-done(((bf16[64,2176]{1,0:T(8,128)(2,1)}), bf16[2048,2176]{1,0:T(8,128)(2,1)}) %all-gather.5.cloned.1.call-update) | async-done | bytes 8912912 | tf_op jit(solution)/shard_map/all_gather | solution.py:287
  182.0 6.8 %shard_map.104 = (bf16[3,384,256]{2,1,0:T(8,128)(2,1)S(1)}, bf16[4,384,256]{2,1,0:T(8,128)(2,1)S(1)}, bf16[4,256,768]{2,1,0:T(8,128)(2,1)S(1)}) custom-call(s32[3]{0:T(128)S(1)} %pad_add_fusion.scal, bf16[4,384,512]{2,1,0:T(8,128)(2,1)} %copy-done, f32[384,128]{1,0:T(8,128)S(1)} %get-tuple-element.18.scale, ...), custom_call_target="tpu_custom_call" | custom-call | flops 2768240640 | bytes 8650752 | tf_op jit(solution)/shard_map/pallas_call | solution.py:341
  188.9 2.8 %collective-permute-start.4 = (bf16[4,384,256]{2,1,0:T(8,128)(2,1)S(1)}, bf16[4,384,256]{2,1,0:T(8,128)(2,1)S(1)}, u32[]{:S(2)}, u32[]{:S(2)}) collective-permute-start(bf16[4,384,256]{2,1,0:T(8,128)(2,1)S(1)} %get-tuple-element.22), channel_id=1, source_target_pairs={{0,1},{1,0},{2,3},{3,2},{4,5},{5,4},{6,7},{7,6},{8,9},{9,8},{10,11... | collective-permute-start | bytes 2359304 | tf_op jit(solution)/shard_map/ppermute | solution.py:232
  191.7 0.8 shard_map.105
  192.5 1.1 collective-permute-done.4
  193.6 0.3 add_convert_fusion
  193.9 15.4 %all_to_all.5 = bf16[4,384,256]{2,1,0:T(8,128)(2,1)S(1)} all-to-all(bf16[4,384,256]{2,1,0:T(8,128)(2,1)S(1)} %add_convert_fusion), channel_id=1, replica_groups=mesh['grp'=2,'fs'=32,'x'=4,'core'=2] {'x'}, dimensions={0} | all-to-all | bytes 1572864 | tf_op jit(solution)/shard_map/all_to_all | solution.py:368
  209.4 0.7 fusion
  (22 shorter events, 0.3 us)
Async XLA Ops:
  6.5 61.6 %copy-start.7 = (bf16[32,256]{1,0:T(8,128)(2,1)S(1)}, bf16[32,256]{1,0:T(8,128)(2,1)}, u32[]{:S(2)}) copy-start(bf16[32,256]{1,0:T(8,128)(2,1)} %param.15) | copy-start | bytes 49156
  6.5 61.6 %copy-start.6 = (bf16[64,128]{1,0:T(8,128)(2,1)S(1)}, bf16[64,128]{1,0:T(8,128)(2,1)}, u32[]{:S(2)}) copy-start(bf16[64,128]{1,0:T(8,128)(2,1)} %param.12) | copy-start | bytes 49156
  6.6 126.0 %copy-start.2 = (bf16[1,128,128]{2,1,0:T(8,128)(2,1)S(1)}, bf16[1,128,128]{2,1,0:T(8,128)(2,1)}, u32[]{:S(2)}) copy-start(bf16[1,128,128]{2,1,0:T(8,128)(2,1)} %pool_weight.1) | copy-start | bytes 98308
  6.6 126.0 %copy-start.4 = (f32[128]{0:T(128)S(1)}, f32[128]{0:T(128)}, u32[]{:S(2)}) copy-start(f32[128]{0:T(128)} %param.14) | copy-start | bytes 1540
  6.6 175.5 %all-gather.5.cloned.1.call-start = ((), (), s32[]{:S(2)}) async-start(), calls=%async_computation.1 | async-start | bytes 9191424 | tf_op jit(solution)/shard_map/all_gather | solution.py:287
  8.7 1.6 collective-permute-start.3
  10.3 0.7 copy-start.5
  23.3 109.3 %collective-permute-start = (bf16[4,400,256]{2,1,0:T(8,128)(2,1)S(1)}, bf16[4,400,256]{2,1,0:T(8,128)(2,1)S(1)}, u32[]{:S(2)}, u32[]{:S(2)}) collective-permute-start(bf16[4,400,256]{2,1,0:T(8,128)(2,1)S(1)} %bitcast.15), channel_id=1, source_target_pairs={{0,1},{1,0},{2,3},{3,2},{4,5},{5,4},{6,7},{7,6},{8,9},{9,8},{10,11... | collective-permute-start | bytes 2457608 | tf_op jit(solution)/shard_map/ppermute | solution.py:232
  121.9 10.7 %collective-permute-start.1 = (bf16[2048,128]{1,0:T(8,128)(2,1)S(1)}, bf16[2048,128]{1,0:T(8,128)(2,1)S(1)}, u32[]{:S(2)}, u32[]{:S(2)}) collective-permute-start(bf16[2048,128]{1,0:T(8,128)(2,1)S(1)} %all_gather.26.mine), channel_id=1, source_target_pairs={{0,256},{256,0},{1,257},{257,1},{2,258},{258,2},{3,259},{259,3},{4... | collective-permute-start | bytes 1572872 | tf_op jit(solution)/shard_map/ppermute | solution.py:299
  132.6 26.1 %copy-start.1 = (bf16[1,384,256]{2,1,0:T(8,128)(2,1)S(1)}, bf16[1,384,256]{2,1,0:T(8,128)(2,1)}, u32[]{:S(2)}) copy-start(bf16[1,384,256]{2,1,0:T(8,128)(2,1)} %param.10) | copy-start | bytes 589828
  132.6 26.1 %copy-start.3 = (f32[256]{0:T(256)S(1)}, f32[256]{0:T(256)}, u32[]{:S(2)}) copy-start(f32[256]{0:T(256)} %param.16) | copy-start | bytes 3076
  172.0 5.6 %collective-permute-start.2 = (bf16[4,384,256]{2,1,0:T(8,128)(2,1)S(1)}, bf16[4,384,256]{2,1,0:T(8,128)(2,1)S(1)}, u32[]{:S(2)}, u32[]{:S(2)}) collective-permute-start(bf16[4,384,256]{2,1,0:T(8,128)(2,1)S(1)} %bitcast.20), channel_id=1, source_target_pairs={{0,1},{1,0},{2,3},{3,2},{4,5},{5,4},{6,7},{7,6},{8,9},{9,8},{10,11... | collective-permute-start | bytes 2359304 | tf_op jit(solution)/shard_map/ppermute | solution.py:232
  178.7 1.1 copy-start
  188.9 4.7 %collective-permute-start.4 = (bf16[4,384,256]{2,1,0:T(8,128)(2,1)S(1)}, bf16[4,384,256]{2,1,0:T(8,128)(2,1)S(1)}, u32[]{:S(2)}, u32[]{:S(2)}) collective-permute-start(bf16[4,384,256]{2,1,0:T(8,128)(2,1)S(1)} %get-tuple-element.22), channel_id=1, source_target_pairs={{0,1},{1,0},{2,3},{3,2},{4,5},{5,4},{6,7},{7,6},{8,9},{9,8},{10,11... | collective-permute-start | bytes 2359304 | tf_op jit(solution)/shard_map/ppermute | solution.py:232
Sparse Core Ops, SparseCore 0:
  11.2 170.7 all-gather.4

commit v6 on v5

--- a/solution.py
+++ b/solution.py
@@ -148,6 +148,10 @@
     scale[...] = jnp.broadcast_to(lax.rsqrt(square / D + EPSILON), scale.shape)
 
 
+def flips(core):
+    return 0, 3 - 2 * core, 1 + 2 * core, 2
+
+
 def hidden_kernel(
     scal, features_at, scale, weight, hidden, partial, kept, features, wide, total, sems
 ):
@@ -198,14 +202,17 @@
             turned = pltpu.roll(both, LANES // 2, 1)
             value = jnp.where(lane < LANES // 2, activated(both, turned), 0.0)
         hidden[pair, :, side * LANES : (side + 1) * LANES] = value.astype(BF16)
-    for chip in range(chips):
-        theirs = pl.multiple_of((1 - core) * width, width)
+    theirs = pl.ds(pl.multiple_of((1 - core) * width, width), width)
+    mine = pl.ds(pl.multiple_of(core * width, width), width)
+    for place, flip in enumerate(flips(1 - core)):
+        chip = jnp.bitwise_xor(scal[3], flip)
         product = jnp.zeros((length, width), F32)
         for p in range(hidden.shape[0]):
             at = gated + p * 2 * LANES
-            product += dot_t(hidden[p], wide[chip, pl.ds(theirs, width), at : at + 2 * LANES])
-        partial[chip] = product.astype(BF16)
-        kept[chip] = wide[chip, pl.ds(pl.multiple_of(core * width, width), width), gated:]
+            product += dot_t(hidden[p], wide[chip, theirs, at : at + 2 * LANES])
+        partial[place] = product.astype(BF16)
+    for place, flip in enumerate(flips(core)):
+        kept[place] = wide[jnp.bitwise_xor(scal[3], flip), mine, gated:]
 
 
 def down_kernel(hidden, down, partial):
@@ -250,7 +257,9 @@
     chips = lax.axis_size("x")
     group = lax.axis_index("x") * CORES + core
     partner = lax.axis_index("grp") % 2
-    scal = jnp.stack([core, jnp.left_shift(1, group % 4), partner]).astype(jnp.int32)
+    scal = jnp.stack(
+        [core, jnp.left_shift(1, group % 4), partner, lax.axis_index("x")]
+    ).astype(jnp.int32)
     smem = spec(pltpu.SMEM)
     anywhere = spec(pl.ANY)
     blocks = (units + LANES - 1) // LANES
@@ -364,9 +373,18 @@
         D * units,
         [spec()] * 2,
     )(hidden, down_own)
-    paired = (partial_own + arrived.astype(F32)).astype(BF16)
-    summed = lax.all_to_all(paired, "x", split_axis=0, concat_axis=0, tiled=True)
-    return (mixed + summed.astype(F32).sum(axis=0)).astype(BF16)[None]
+    def exchange(array, step):
+        pairs = [
+            (x * CORES + c, (x ^ flips(c)[step]) * CORES + c)
+            for x in range(chips)
+            for c in range(CORES)
+        ]
+        return lax.ppermute(array, ("x", "core"), pairs).astype(F32)
+
+    paired = partial_own + arrived.astype(F32)
+    halved = paired[:2] + exchange(paired[2:].astype(BF16), 2)
+    last = exchange(halved[1].astype(BF16), 1)
+    return (mixed + (halved[0] + last)).astype(BF16)[None]
 
 
 def solution(mesh):

time: 217 us -> 219 us (level)
  blocking collectives: 118 us -> 102 us
  waiting for transfers between devices: 12.1 us -> 21.8 us
  starting transfers between devices: 56.7 us -> 63.6 us
    all_to_all x1 -> x0, blocking collectives: 15.4 us -> none  [local(): lax.all_to_all(paired, 'x', split_axis=0, concat_axis=0, tiled=True)]
    ppermute x0 -> x2, waiting for transfers between devices: none -> 9.68 us  [exchange(): return lax.ppermute(array, ('x', 'core'), pairs).astype(F32)]
    ppermute x0 -> x2, starting transfers between devices: none -> 6.89 us  [exchange(): return lax.ppermute(array, ('x', 'core'), pairs).astype(F32)]
  transfers between devices with their start and end apart: 6 -> 8, of which waited for: 4 -> 6; matrix products, arithmetic and copies ran while one was open for 0% -> 0% of each run, Pallas kernels for 2% -> 2%
where the time goes in v6:
time: 219 us; the launch traced here: 218 us
  blocking collectives  102 us (47%)
  starting transfers between devices  63.6 us (29%)
  waiting for transfers between devices  21.8 us (10%)
  Pallas kernels  13.9 us (6%)
  between operations  13.6 us (6%)
    all_gather x1, blocking collectives, local(): mine = lax.all_gather(chosen, 'fs', axis=0, tiled=True)  53.8 us
    ppermute x3, starting transfers between devices, swap(): return lax.ppermute(array, 'core', [(0, 1), (1, 0)])  51.4 us
    all_gather x1, blocking collectives, local(): pooled_all = lax.all_gather(pooled, ('x', 'core'), axis=0)  24 us
    all_gather x1, blocking collectives, local(): own = lax.all_gather(sent, 'x', axis=0)  12.2 us
    all_gather x1, blocking collectives, local(): own_two = lax.all_gather(scaled, 'x', axis=0)  12.2 us
    ppermute x2, waiting for transfers between devices, exchange(): return lax.ppermute(array, ('x', 'core'), pairs).astype(F32)  9.68 us
    ppermute x2, starting transfers between devices, exchange(): return lax.ppermute(array, ('x', 'core'), pairs).astype(F32)  6.89 us
    ppermute x1, waiting for transfers between devices, local(): theirs = lax.ppermute(mine, 'grp', [(i, i ^ 1) for i in range(groups)])  6.86 us
  transfers between devices with their start and end apart: 8, of which 6 were waited for; matrix products, arithmetic and copies ran while one was open for 0% of the time, Pallas kernels for 2%

profile of v6, /device:TPU:33, one launch (start us, length us, event | category | flops | bytes accessed | tf_op | source)
XLA Modules:
  0.0 218.1 jit_solution(15204514939457685986)
XLA Ops:
  6.6 2.0 shard_map.100
  8.6 1.6 collective-permute-start.3
  11.0 12.2 %all-gather = bf16[1600,256]{1,0:T(8,128)(2,1)S(1)} all-gather(bf16[400,256]{1,0:T(8,128)(2,1)} %get-tuple-element.14), channel_id=2, replica_groups=mesh['grp'=2,'fs'=32,'x'=4,'core'=2] {'x'}, dimensions={0}, use_global_device_ids=true | all-gather | bytes 1024000 | tf_op jit(solution)/shard_map/all_gather | solution.py:300
  23.2 44.8 %collective-permute-start = (bf16[4,400,256]{2,1,0:T(8,128)(2,1)S(1)}, bf16[4,400,256]{2,1,0:T(8,128)(2,1)S(1)}, u32[]{:S(2)}, u32[]{:S(2)}) collective-permute-start(bf16[4,400,256]{2,1,0:T(8,128)(2,1)S(1)} %bitcast.28), channel_id=1, source_target_pairs={{0,1},{1,0},{2,3},{3,2},{4,5},{5,4},{6,7},{7,6},{8,9},{9,8},{10,11... | collective-permute-start | bytes 2457608 | tf_op jit(solution)/shard_map/ppermute | solution.py:239
  68.1 53.8 %all_gather.26.mine = bf16[2048,128]{1,0:T(8,128)(2,1)S(1)} all-gather(bf16[64,128]{1,0:T(8,128)(2,1)S(1)} %maximum_select_fusion), channel_id=1, replica_groups=mesh['grp'=2,'fs'=32,'x'=4,'core'=2] {'fs'}, dimensions={0}, use_global_device_ids=true | all-gather | bytes 540672 | tf_op jit(solution)/shard_map/all_gather | solution.py:306
  121.9 3.7 %collective-permute-start.1 = (bf16[2048,128]{1,0:T(8,128)(2,1)S(1)}, bf16[2048,128]{1,0:T(8,128)(2,1)S(1)}, u32[]{:S(2)}, u32[]{:S(2)}) collective-permute-start(bf16[2048,128]{1,0:T(8,128)(2,1)S(1)} %all_gather.26.mine), channel_id=1, source_target_pairs={{0,256},{256,0},{1,257},{257,1},{2,258},{258,2},{3,259},{259,3},{4... | collective-permute-start | bytes 1572872 | tf_op jit(solution)/shard_map/ppermute | solution.py:308
  125.7 6.9 %collective-permute-done.1.theirs = bf16[2048,128]{1,0:T(8,128)(2,1)S(1)} collective-permute-done((bf16[2048,128]{1,0:T(8,128)(2,1)S(1)}, bf16[2048,128]{1,0:T(8,128)(2,1)S(1)}, u32[]{:S(2)}, u32[]{:S(2)}) %collective-permute-start.1) | collective-permute-done | bytes 524320 | tf_op jit(solution)/shard_map/ppermute | solution.py:308
  132.6 2.0 shard_map.101
  134.6 24.0 %all-gather.1 = bf16[3072,128]{1,0:T(8,128)(2,1)S(1)} all-gather(bf16[384,128]{1,0:T(8,128)(2,1)S(1)} %shard_map.101), channel_id=3, replica_groups=mesh['grp'=2,'fs'=32,'x'=4,'core'=2] {'x','core'}, dimensions={0}, use_global_device_ids=true | all-gather | bytes 884736 | tf_op jit(solution)/shard_map/all_gather | solution.py:317
  158.6 1.2 shard_map.102
  159.8 12.2 %all-gather.2 = bf16[1536,256]{1,0:T(8,128)(2,1)S(1)} all-gather(bf16[384,256]{1,0:T(8,128)(2,1)S(1)} %get-tuple-element.16), channel_id=4, replica_groups=mesh['grp'=2,'fs'=32,'x'=4,'core'=2] {'x'}, dimensions={0}, use_global_device_ids=true | all-gather | bytes 983040 | tf_op jit(solution)/shard_map/all_gather | solution.py:337
  172.0 3.7 %collective-permute-start.2 = (bf16[4,384,256]{2,1,0:T(8,128)(2,1)S(1)}, bf16[4,384,256]{2,1,0:T(8,128)(2,1)S(1)}, u32[]{:S(2)}, u32[]{:S(2)}) collective-permute-start(bf16[4,384,256]{2,1,0:T(8,128)(2,1)S(1)} %bitcast.33), channel_id=1, source_target_pairs={{0,1},{1,0},{2,3},{3,2},{4,5},{5,4},{6,7},{7,6},{8,9},{9,8},{10,11... | collective-permute-start | bytes 2359304 | tf_op jit(solution)/shard_map/ppermute | solution.py:239
  175.7 1.9 collective-permute-done.2.other
  177.6 1.1 shard_map.103
  178.7 1.1 copy-done
  179.8 2.2 %all-gather.5.cloned.1.call-done.weight = bf16[2048,2176]{1,0:T(8,128)(2,1)} async-done(((bf16[64,2176]{1,0:T(8,128)(2,1)}), bf16[2048,2176]{1,0:T(8,128)(2,1)}) %all-gather.5.cloned.1.call-update) | async-done | bytes 8912912 | tf_op jit(solution)/shard_map/all_gather | solution.py:296
  182.0 6.8 %shard_map.104 = (bf16[3,384,256]{2,1,0:T(8,128)(2,1)S(1)}, bf16[4,384,256]{2,1,0:T(8,128)(2,1)S(1)}, bf16[4,256,768]{2,1,0:T(8,128)(2,1)S(1)}) custom-call(s32[4]{0:T(128)S(1)} %pad_add_fusion.scal, bf16[4,384,512]{2,1,0:T(8,128)(2,1)} %copy-done, f32[384,128]{1,0:T(8,128)S(1)} %get-tuple-element.18.scale, ...), custom_call_target="tpu_custom_call" | custom-call | flops 2768240640 | bytes 8650752 | tf_op jit(solution)/shard_map/pallas_call | solution.py:350
  188.8 2.8 %collective-permute-start.4 = (bf16[4,384,256]{2,1,0:T(8,128)(2,1)S(1)}, bf16[4,384,256]{2,1,0:T(8,128)(2,1)S(1)}, u32[]{:S(2)}, u32[]{:S(2)}) collective-permute-start(bf16[4,384,256]{2,1,0:T(8,128)(2,1)S(1)} %get-tuple-element.22), channel_id=1, source_target_pairs={{0,1},{1,0},{2,3},{3,2},{4,5},{5,4},{6,7},{7,6},{8,9},{9,8},{10,11... | collective-permute-start | bytes 2359304 | tf_op jit(solution)/shard_map/ppermute | solution.py:239
  191.7 0.8 shard_map.105
  192.5 1.1 collective-permute-done.4
  193.8 4.7 %collective-permute-start.5 = (bf16[2,384,256]{2,1,0:T(8,128)(2,1)S(1)}, bf16[2,384,256]{2,1,0:T(8,128)(2,1)S(1)}, u32[]{:S(2)}, u32[]{:S(2)}) collective-permute-start(bf16[2,384,256]{2,1,0:T(8,128)(2,1)S(1)} %slice.36), channel_id=1, source_target_pairs={{0,2},{1,7},{2,0},{3,5},{4,6},{5,3},{6,4},{7,1},{8,10},{9,15},{10,... | collective-permute-start | bytes 1179656 | tf_op jit(solution)/shard_map/ppermute | solution.py:382
  198.5 5.2 %collective-permute-done.5 = bf16[2,384,256]{2,1,0:T(8,128)(2,1)S(1)} collective-permute-done((bf16[2,384,256]{2,1,0:T(8,128)(2,1)S(1)}, bf16[2,384,256]{2,1,0:T(8,128)(2,1)S(1)}, u32[]{:S(2)}, u32[]{:S(2)}) %collective-permute-start.5) | collective-permute-done | bytes 393248 | tf_op jit(solution)/shard_map/ppermute | solution.py:382
  203.8 2.2 %collective-permute-start.6 = (bf16[384,256]{1,0:T(8,128)(2,1)S(1)}, bf16[384,256]{1,0:T(8,128)(2,1)S(1)}, u32[]{:S(2)}, u32[]{:S(2)}) collective-permute-start(bf16[384,256]{1,0:T(8,128)(2,1)S(1)} %fusion.4), channel_id=1, source_target_pairs={{0,6},{1,3},{2,4},{3,1},{4,2},{5,7},{6,0},{7,5},{8,14},{9,11},{10,... | collective-permute-start | bytes 589832 | tf_op jit(solution)/shard_map/ppermute | solution.py:382
  206.0 4.5 %collective-permute-done.6 = bf16[384,256]{1,0:T(8,128)(2,1)S(1)} collective-permute-done((bf16[384,256]{1,0:T(8,128)(2,1)S(1)}, bf16[384,256]{1,0:T(8,128)(2,1)S(1)}, u32[]{:S(2)}, u32[]{:S(2)}) %collective-permute-start.6) | collective-permute-done | bytes 196640 | tf_op jit(solution)/shard_map/ppermute | solution.py:382
  (27 shorter events, 2.1 us)
Async XLA Ops:
  6.5 61.5 %copy-start.7 = (bf16[32,256]{1,0:T(8,128)(2,1)S(1)}, bf16[32,256]{1,0:T(8,128)(2,1)}, u32[]{:S(2)}) copy-start(bf16[32,256]{1,0:T(8,128)(2,1)} %param.15) | copy-start | bytes 49156
  6.5 61.5 %copy-start.6 = (bf16[64,128]{1,0:T(8,128)(2,1)S(1)}, bf16[64,128]{1,0:T(8,128)(2,1)}, u32[]{:S(2)}) copy-start(bf16[64,128]{1,0:T(8,128)(2,1)} %param.12) | copy-start | bytes 49156
  6.6 126.0 %copy-start.2 = (bf16[1,128,128]{2,1,0:T(8,128)(2,1)S(1)}, bf16[1,128,128]{2,1,0:T(8,128)(2,1)}, u32[]{:S(2)}) copy-start(bf16[1,128,128]{2,1,0:T(8,128)(2,1)} %pool_weight.1) | copy-start | bytes 98308
  6.6 126.0 %copy-start.4 = (f32[128]{0:T(128)S(1)}, f32[128]{0:T(128)}, u32[]{:S(2)}) copy-start(f32[128]{0:T(128)} %param.14) | copy-start | bytes 1540
  6.6 175.5 %all-gather.5.cloned.1.call-start = ((), (), s32[]{:S(2)}) async-start(), calls=%async_computation | async-start | bytes 9191424 | tf_op jit(solution)/shard_map/all_gather | solution.py:296
  8.6 1.6 collective-permute-start.3
  10.3 0.7 copy-start.5
  23.2 109.3 %collective-permute-start = (bf16[4,400,256]{2,1,0:T(8,128)(2,1)S(1)}, bf16[4,400,256]{2,1,0:T(8,128)(2,1)S(1)}, u32[]{:S(2)}, u32[]{:S(2)}) collective-permute-start(bf16[4,400,256]{2,1,0:T(8,128)(2,1)S(1)} %bitcast.28), channel_id=1, source_target_pairs={{0,1},{1,0},{2,3},{3,2},{4,5},{5,4},{6,7},{7,6},{8,9},{9,8},{10,11... | collective-permute-start | bytes 2457608 | tf_op jit(solution)/shard_map/ppermute | solution.py:239
  121.9 10.7 %collective-permute-start.1 = (bf16[2048,128]{1,0:T(8,128)(2,1)S(1)}, bf16[2048,128]{1,0:T(8,128)(2,1)S(1)}, u32[]{:S(2)}, u32[]{:S(2)}) collective-permute-start(bf16[2048,128]{1,0:T(8,128)(2,1)S(1)} %all_gather.26.mine), channel_id=1, source_target_pairs={{0,256},{256,0},{1,257},{257,1},{2,258},{258,2},{3,259},{259,3},{4... | collective-permute-start | bytes 1572872 | tf_op jit(solution)/shard_map/ppermute | solution.py:308
  132.5 26.1 %copy-start.1 = (bf16[1,384,256]{2,1,0:T(8,128)(2,1)S(1)}, bf16[1,384,256]{2,1,0:T(8,128)(2,1)}, u32[]{:S(2)}) copy-start(bf16[1,384,256]{2,1,0:T(8,128)(2,1)} %param.10) | copy-start | bytes 589828
  132.6 26.0 %copy-start.3 = (f32[256]{0:T(256)S(1)}, f32[256]{0:T(256)}, u32[]{:S(2)}) copy-start(f32[256]{0:T(256)} %param.16) | copy-start | bytes 3076
  172.0 5.6 %collective-permute-start.2 = (bf16[4,384,256]{2,1,0:T(8,128)(2,1)S(1)}, bf16[4,384,256]{2,1,0:T(8,128)(2,1)S(1)}, u32[]{:S(2)}, u32[]{:S(2)}) collective-permute-start(bf16[4,384,256]{2,1,0:T(8,128)(2,1)S(1)} %bitcast.33), channel_id=1, source_target_pairs={{0,1},{1,0},{2,3},{3,2},{4,5},{5,4},{6,7},{7,6},{8,9},{9,8},{10,11... | collective-permute-start | bytes 2359304 | tf_op jit(solution)/shard_map/ppermute | solution.py:239
  178.7 1.1 copy-start
  188.8 4.7 %collective-permute-start.4 = (bf16[4,384,256]{2,1,0:T(8,128)(2,1)S(1)}, bf16[4,384,256]{2,1,0:T(8,128)(2,1)S(1)}, u32[]{:S(2)}, u32[]{:S(2)}) collective-permute-start(bf16[4,384,256]{2,1,0:T(8,128)(2,1)S(1)} %get-tuple-element.22), channel_id=1, source_target_pairs={{0,1},{1,0},{2,3},{3,2},{4,5},{5,4},{6,7},{7,6},{8,9},{9,8},{10,11... | collective-permute-start | bytes 2359304 | tf_op jit(solution)/shard_map/ppermute | solution.py:239
  193.8 9.8 %collective-permute-start.5 = (bf16[2,384,256]{2,1,0:T(8,128)(2,1)S(1)}, bf16[2,384,256]{2,1,0:T(8,128)(2,1)S(1)}, u32[]{:S(2)}, u32[]{:S(2)}) collective-permute-start(bf16[2,384,256]{2,1,0:T(8,128)(2,1)S(1)} %slice.36), channel_id=1, source_target_pairs={{0,2},{1,7},{2,0},{3,5},{4,6},{5,3},{6,4},{7,1},{8,10},{9,15},{10,... | collective-permute-start | bytes 1179656 | tf_op jit(solution)/shard_map/ppermute | solution.py:382
  203.8 6.7 %collective-permute-start.6 = (bf16[384,256]{1,0:T(8,128)(2,1)S(1)}, bf16[384,256]{1,0:T(8,128)(2,1)S(1)}, u32[]{:S(2)}, u32[]{:S(2)}) collective-permute-start(bf16[384,256]{1,0:T(8,128)(2,1)S(1)} %fusion.4), channel_id=1, source_target_pairs={{0,6},{1,3},{2,4},{3,1},{4,2},{5,7},{6,0},{7,5},{8,14},{9,11},{10,... | collective-permute-start | bytes 589832 | tf_op jit(solution)/shard_map/ppermute | solution.py:382
Sparse Core Ops, SparseCore 0:
  11.2 170.8 all-gather.4

commit v7 on v6

--- a/solution.py
+++ b/solution.py
@@ -148,10 +148,6 @@
     scale[...] = jnp.broadcast_to(lax.rsqrt(square / D + EPSILON), scale.shape)
 
 
-def flips(core):
-    return 0, 3 - 2 * core, 1 + 2 * core, 2
-
-
 def hidden_kernel(
     scal, features_at, scale, weight, hidden, partial, kept, features, wide, total, sems
 ):
@@ -204,15 +200,14 @@
         hidden[pair, :, side * LANES : (side + 1) * LANES] = value.astype(BF16)
     theirs = pl.ds(pl.multiple_of((1 - core) * width, width), width)
     mine = pl.ds(pl.multiple_of(core * width, width), width)
-    for place, flip in enumerate(flips(1 - core)):
-        chip = jnp.bitwise_xor(scal[3], flip)
+    for place in range(chips):
+        chip = lax.rem(scal[3] + place, chips)
         product = jnp.zeros((length, width), F32)
         for p in range(hidden.shape[0]):
             at = gated + p * 2 * LANES
             product += dot_t(hidden[p], wide[chip, theirs, at : at + 2 * LANES])
         partial[place] = product.astype(BF16)
-    for place, flip in enumerate(flips(core)):
-        kept[place] = wide[jnp.bitwise_xor(scal[3], flip), mine, gated:]
+        kept[place] = wide[chip, mine, gated:]
 
 
 def down_kernel(hidden, down, partial):
@@ -373,18 +368,12 @@
         D * units,
         [spec()] * 2,
     )(hidden, down_own)
-    def exchange(array, step):
-        pairs = [
-            (x * CORES + c, (x ^ flips(c)[step]) * CORES + c)
-            for x in range(chips)
-            for c in range(CORES)
-        ]
-        return lax.ppermute(array, ("x", "core"), pairs).astype(F32)
-
     paired = partial_own + arrived.astype(F32)
-    halved = paired[:2] + exchange(paired[2:].astype(BF16), 2)
-    last = exchange(halved[1].astype(BF16), 1)
-    return (mixed + (halved[0] + last)).astype(BF16)[None]
+    total = paired[0]
+    for k in (1, chips - 1, *range(2, chips - 1)):
+        onward = [(x, (x + k) % chips) for x in range(chips)]
+        total = total + lax.ppermute(paired[k].astype(BF16), "x", onward).astype(F32)
+    return (mixed + total).astype(BF16)[None]
 
 
 def solution(mesh):

time: 219 us -> 218 us (level)
  waiting for transfers between devices: 21.8 us -> 18.2 us
  starting transfers between devices: 63.6 us -> 66.8 us
    ppermute x2 -> x3, waiting for transfers between devices: 9.68 us -> 6.09 us  [local(): lax.ppermute(paired[k].astype(BF16), 'x', onward).astype(F32)]
    ppermute x2 -> x3, starting transfers between devices: 6.89 us -> 10.1 us  [local(): lax.ppermute(paired[k].astype(BF16), 'x', onward).astype(F32)]
  transfers between devices with their start and end apart: 8 -> 9, of which waited for: 6 -> 6; matrix products, arithmetic and copies ran while one was open for 0% -> 0% of each run, Pallas kernels for 2% -> 2%
where the time goes in v7:
time: 218 us
  blocking collectives  102 us (47%)
  starting transfers between devices  66.8 us (31%)
  waiting for transfers between devices  18.2 us (8%)
  Pallas kernels  13.9 us (6%)
  between operations  13.6 us (6%)
    all_gather x1, blocking collectives, local(): mine = lax.all_gather(chosen, 'fs', axis=0, tiled=True)  53.8 us
    ppermute x3, starting transfers between devices, swap(): return lax.ppermute(array, 'core', [(0, 1), (1, 0)])  51.4 us
    all_gather x1, blocking collectives, local(): pooled_all = lax.all_gather(pooled, ('x', 'core'), axis=0)  24 us
    all_gather x1, blocking collectives, local(): own = lax.all_gather(sent, 'x', axis=0)  12.2 us
    all_gather x1, blocking collectives, local(): own_two = lax.all_gather(scaled, 'x', axis=0)  12.2 us
    ppermute x3, starting transfers between devices, local(): lax.ppermute(paired[k].astype(BF16), 'x', onward).astype(F32)  10.1 us
    pallas_call x1, Pallas kernels, local(): call(hidden_kernel, (jax.ShapeDtypeStruct((blocks // 2, length, 2 * LANES...  6.87 us
    ppermute x1, waiting for transfers between devices, local(): theirs = lax.ppermute(mine, 'grp', [(i, i ^ 1) for i in range(groups)])  6.86 us
  transfers between devices with their start and end apart: 9, of which 6 were waited for; matrix products, arithmetic and copies ran while one was open for 0% of the time, Pallas kernels for 2%

profile of v7, /device:TPU:33, one launch (start us, length us, event | category | flops | bytes accessed | tf_op | source)
XLA Modules:
  0.0 217.8 jit_solution(2978388836923855267)
XLA Ops:
  6.6 2.0 shard_map.100
  8.6 1.6 collective-permute-start.3
  11.0 12.2 %all-gather = bf16[1600,256]{1,0:T(8,128)(2,1)S(1)} all-gather(bf16[400,256]{1,0:T(8,128)(2,1)} %get-tuple-element.14), channel_id=2, replica_groups=mesh['grp'=2,'fs'=32,'x'=4,'core'=2] {'x'}, dimensions={0}, use_global_device_ids=true | all-gather | bytes 1024000 | tf_op jit(solution)/shard_map/all_gather | solution.py:295
  23.2 44.8 %collective-permute-start = (bf16[4,400,256]{2,1,0:T(8,128)(2,1)S(1)}, bf16[4,400,256]{2,1,0:T(8,128)(2,1)S(1)}, u32[]{:S(2)}, u32[]{:S(2)}) collective-permute-start(bf16[4,400,256]{2,1,0:T(8,128)(2,1)S(1)} %bitcast.36), channel_id=1, source_target_pairs={{0,1},{1,0},{2,3},{3,2},{4,5},{5,4},{6,7},{7,6},{8,9},{9,8},{10,11... | collective-permute-start | bytes 2457608 | tf_op jit(solution)/shard_map/ppermute | solution.py:234
  68.1 53.8 %all_gather.26.mine = bf16[2048,128]{1,0:T(8,128)(2,1)S(1)} all-gather(bf16[64,128]{1,0:T(8,128)(2,1)S(1)} %maximum_select_fusion), channel_id=1, replica_groups=mesh['grp'=2,'fs'=32,'x'=4,'core'=2] {'fs'}, dimensions={0}, use_global_device_ids=true | all-gather | bytes 540672 | tf_op jit(solution)/shard_map/all_gather | solution.py:301
  121.9 3.7 %collective-permute-start.1 = (bf16[2048,128]{1,0:T(8,128)(2,1)S(1)}, bf16[2048,128]{1,0:T(8,128)(2,1)S(1)}, u32[]{:S(2)}, u32[]{:S(2)}) collective-permute-start(bf16[2048,128]{1,0:T(8,128)(2,1)S(1)} %all_gather.26.mine), channel_id=1, source_target_pairs={{0,256},{256,0},{1,257},{257,1},{2,258},{258,2},{3,259},{259,3},{4... | collective-permute-start | bytes 1572872 | tf_op jit(solution)/shard_map/ppermute | solution.py:303
  125.7 6.9 %collective-permute-done.1.theirs = bf16[2048,128]{1,0:T(8,128)(2,1)S(1)} collective-permute-done((bf16[2048,128]{1,0:T(8,128)(2,1)S(1)}, bf16[2048,128]{1,0:T(8,128)(2,1)S(1)}, u32[]{:S(2)}, u32[]{:S(2)}) %collective-permute-start.1) | collective-permute-done | bytes 524320 | tf_op jit(solution)/shard_map/ppermute | solution.py:303
  132.6 2.0 shard_map.101
  134.6 24.0 %all-gather.1 = bf16[3072,128]{1,0:T(8,128)(2,1)S(1)} all-gather(bf16[384,128]{1,0:T(8,128)(2,1)S(1)} %shard_map.101), channel_id=3, replica_groups=mesh['grp'=2,'fs'=32,'x'=4,'core'=2] {'x','core'}, dimensions={0}, use_global_device_ids=true | all-gather | bytes 884736 | tf_op jit(solution)/shard_map/all_gather | solution.py:312
  158.6 1.2 shard_map.102
  159.8 12.2 %all-gather.2 = bf16[1536,256]{1,0:T(8,128)(2,1)S(1)} all-gather(bf16[384,256]{1,0:T(8,128)(2,1)S(1)} %get-tuple-element.16), channel_id=4, replica_groups=mesh['grp'=2,'fs'=32,'x'=4,'core'=2] {'x'}, dimensions={0}, use_global_device_ids=true | all-gather | bytes 983040 | tf_op jit(solution)/shard_map/all_gather | solution.py:332
  172.0 3.7 %collective-permute-start.2 = (bf16[4,384,256]{2,1,0:T(8,128)(2,1)S(1)}, bf16[4,384,256]{2,1,0:T(8,128)(2,1)S(1)}, u32[]{:S(2)}, u32[]{:S(2)}) collective-permute-start(bf16[4,384,256]{2,1,0:T(8,128)(2,1)S(1)} %bitcast.41), channel_id=1, source_target_pairs={{0,1},{1,0},{2,3},{3,2},{4,5},{5,4},{6,7},{7,6},{8,9},{9,8},{10,11... | collective-permute-start | bytes 2359304 | tf_op jit(solution)/shard_map/ppermute | solution.py:234
  175.7 1.9 collective-permute-done.2.other
  177.6 1.1 shard_map.103
  178.7 1.1 copy-done
  179.8 2.2 %all-gather.5.cloned.1.call-done.weight = bf16[2048,2176]{1,0:T(8,128)(2,1)} async-done(((bf16[64,2176]{1,0:T(8,128)(2,1)}), bf16[2048,2176]{1,0:T(8,128)(2,1)}) %all-gather.5.cloned.1.call-update) | async-done | bytes 8912912 | tf_op jit(solution)/shard_map/all_gather | solution.py:291
  182.0 6.9 %shard_map.104 = (bf16[3,384,256]{2,1,0:T(8,128)(2,1)S(1)}, bf16[4,384,256]{2,1,0:T(8,128)(2,1)S(1)}, bf16[4,256,768]{2,1,0:T(8,128)(2,1)S(1)}) custom-call(s32[4]{0:T(128)S(1)} %pad_add_fusion.scal, bf16[4,384,512]{2,1,0:T(8,128)(2,1)} %copy-done, f32[384,128]{1,0:T(8,128)S(1)} %get-tuple-element.18.scale, ...), custom_call_target="tpu_custom_call" | custom-call | flops 2768240640 | bytes 8650752 | tf_op jit(solution)/shard_map/pallas_call | solution.py:345
  188.9 2.8 %collective-permute-start.4 = (bf16[4,384,256]{2,1,0:T(8,128)(2,1)S(1)}, bf16[4,384,256]{2,1,0:T(8,128)(2,1)S(1)}, u32[]{:S(2)}, u32[]{:S(2)}) collective-permute-start(bf16[4,384,256]{2,1,0:T(8,128)(2,1)S(1)} %get-tuple-element.22), channel_id=1, source_target_pairs={{0,1},{1,0},{2,3},{3,2},{4,5},{5,4},{6,7},{7,6},{8,9},{9,8},{10,11... | collective-permute-start | bytes 2359304 | tf_op jit(solution)/shard_map/ppermute | solution.py:234
  192.5 1.1 collective-permute-done.4
  194.0 4.7 %collective-permute-start.7 = (bf16[384,256]{1,0:T(8,128)(2,1)S(1)}, bf16[384,256]{1,0:T(8,128)(2,1)S(1)}, u32[]{:S(2)}, u32[]{:S(2)}) collective-permute-start(bf16[384,256]{1,0:T(8,128)(2,1)S(1)} %get-tuple-element.26), channel_id=1, source_target_pairs={{0,4},{2,6},{4,0},{6,2},{1,5},{3,7},{5,1},{7,3},{8,12},{10,14},{12... | collective-permute-start | bytes 589832 | tf_op jit(solution)/shard_map/ppermute | solution.py:375
  198.7 2.8 %collective-permute-start.6 = (bf16[384,256]{1,0:T(8,128)(2,1)S(1)}, bf16[384,256]{1,0:T(8,128)(2,1)S(1)}, u32[]{:S(2)}, u32[]{:S(2)}) collective-permute-start(bf16[384,256]{1,0:T(8,128)(2,1)S(1)} %get-tuple-element.27), channel_id=1, source_target_pairs={{0,6},{2,0},{4,2},{6,4},{1,7},{3,1},{5,3},{7,5},{8,14},{10,8},{12,... | collective-permute-start | bytes 589832 | tf_op jit(solution)/shard_map/ppermute | solution.py:375
  201.5 2.6 %collective-permute-start.5 = (bf16[384,256]{1,0:T(8,128)(2,1)S(1)}, bf16[384,256]{1,0:T(8,128)(2,1)S(1)}, u32[]{:S(2)}, u32[]{:S(2)}) collective-permute-start(bf16[384,256]{1,0:T(8,128)(2,1)S(1)} %get-tuple-element.25), channel_id=1, source_target_pairs={{0,2},{2,4},{4,6},{6,0},{1,3},{3,5},{5,7},{7,1},{8,10},{10,12},{12... | collective-permute-start | bytes 589832 | tf_op jit(solution)/shard_map/ppermute | solution.py:375
  204.1 4.0 %collective-permute-done.6 = bf16[384,256]{1,0:T(8,128)(2,1)S(1)} collective-permute-done((bf16[384,256]{1,0:T(8,128)(2,1)S(1)}, bf16[384,256]{1,0:T(8,128)(2,1)S(1)}, u32[]{:S(2)}, u32[]{:S(2)}) %collective-permute-start.6) | collective-permute-done | bytes 196640 | tf_op jit(solution)/shard_map/ppermute | solution.py:375
  208.0 2.1 collective-permute-done.5
  (27 shorter events, 2.8 us)
Async XLA Ops:
  6.5 61.5 %copy-start.7 = (bf16[32,256]{1,0:T(8,128)(2,1)S(1)}, bf16[32,256]{1,0:T(8,128)(2,1)}, u32[]{:S(2)}) copy-start(bf16[32,256]{1,0:T(8,128)(2,1)} %param.15) | copy-start | bytes 49156
  6.5 61.5 %copy-start.6 = (bf16[64,128]{1,0:T(8,128)(2,1)S(1)}, bf16[64,128]{1,0:T(8,128)(2,1)}, u32[]{:S(2)}) copy-start(bf16[64,128]{1,0:T(8,128)(2,1)} %param.12) | copy-start | bytes 49156
  6.6 126.0 %copy-start.2 = (bf16[1,128,128]{2,1,0:T(8,128)(2,1)S(1)}, bf16[1,128,128]{2,1,0:T(8,128)(2,1)}, u32[]{:S(2)}) copy-start(bf16[1,128,128]{2,1,0:T(8,128)(2,1)} %pool_weight.1) | copy-start | bytes 98308
  6.6 126.0 %copy-start.4 = (f32[128]{0:T(128)S(1)}, f32[128]{0:T(128)}, u32[]{:S(2)}) copy-start(f32[128]{0:T(128)} %param.14) | copy-start | bytes 1540
  6.6 175.5 %all-gather.5.cloned.1.call-start = ((), (), s32[]{:S(2)}) async-start(), calls=%async_computation | async-start | bytes 9191424 | tf_op jit(solution)/shard_map/all_gather | solution.py:291
  8.6 1.6 collective-permute-start.3
  10.3 0.7 copy-start.5
  23.2 109.3 %collective-permute-start = (bf16[4,400,256]{2,1,0:T(8,128)(2,1)S(1)}, bf16[4,400,256]{2,1,0:T(8,128)(2,1)S(1)}, u32[]{:S(2)}, u32[]{:S(2)}) collective-permute-start(bf16[4,400,256]{2,1,0:T(8,128)(2,1)S(1)} %bitcast.36), channel_id=1, source_target_pairs={{0,1},{1,0},{2,3},{3,2},{4,5},{5,4},{6,7},{7,6},{8,9},{9,8},{10,11... | collective-permute-start | bytes 2457608 | tf_op jit(solution)/shard_map/ppermute | solution.py:234
  121.9 10.7 %collective-permute-start.1 = (bf16[2048,128]{1,0:T(8,128)(2,1)S(1)}, bf16[2048,128]{1,0:T(8,128)(2,1)S(1)}, u32[]{:S(2)}, u32[]{:S(2)}) collective-permute-start(bf16[2048,128]{1,0:T(8,128)(2,1)S(1)} %all_gather.26.mine), channel_id=1, source_target_pairs={{0,256},{256,0},{1,257},{257,1},{2,258},{258,2},{3,259},{259,3},{4... | collective-permute-start | bytes 1572872 | tf_op jit(solution)/shard_map/ppermute | solution.py:303
  132.5 26.1 %copy-start.1 = (bf16[1,384,256]{2,1,0:T(8,128)(2,1)S(1)}, bf16[1,384,256]{2,1,0:T(8,128)(2,1)}, u32[]{:S(2)}) copy-start(bf16[1,384,256]{2,1,0:T(8,128)(2,1)} %param.10) | copy-start | bytes 589828
  132.6 26.0 %copy-start.3 = (f32[256]{0:T(256)S(1)}, f32[256]{0:T(256)}, u32[]{:S(2)}) copy-start(f32[256]{0:T(256)} %param.16) | copy-start | bytes 3076
  172.0 5.6 %collective-permute-start.2 = (bf16[4,384,256]{2,1,0:T(8,128)(2,1)S(1)}, bf16[4,384,256]{2,1,0:T(8,128)(2,1)S(1)}, u32[]{:S(2)}, u32[]{:S(2)}) collective-permute-start(bf16[4,384,256]{2,1,0:T(8,128)(2,1)S(1)} %bitcast.41), channel_id=1, source_target_pairs={{0,1},{1,0},{2,3},{3,2},{4,5},{5,4},{6,7},{7,6},{8,9},{9,8},{10,11... | collective-permute-start | bytes 2359304 | tf_op jit(solution)/shard_map/ppermute | solution.py:234
  178.7 1.2 copy-start
  188.9 4.7 %collective-permute-start.4 = (bf16[4,384,256]{2,1,0:T(8,128)(2,1)S(1)}, bf16[4,384,256]{2,1,0:T(8,128)(2,1)S(1)}, u32[]{:S(2)}, u32[]{:S(2)}) collective-permute-start(bf16[4,384,256]{2,1,0:T(8,128)(2,1)S(1)} %get-tuple-element.22), channel_id=1, source_target_pairs={{0,1},{1,0},{2,3},{3,2},{4,5},{5,4},{6,7},{7,6},{8,9},{9,8},{10,11... | collective-permute-start | bytes 2359304 | tf_op jit(solution)/shard_map/ppermute | solution.py:234
  194.0 10.1 %collective-permute-start.7 = (bf16[384,256]{1,0:T(8,128)(2,1)S(1)}, bf16[384,256]{1,0:T(8,128)(2,1)S(1)}, u32[]{:S(2)}, u32[]{:S(2)}) collective-permute-start(bf16[384,256]{1,0:T(8,128)(2,1)S(1)} %get-tuple-element.26), channel_id=1, source_target_pairs={{0,4},{2,6},{4,0},{6,2},{1,5},{3,7},{5,1},{7,3},{8,12},{10,14},{12... | collective-permute-start | bytes 589832 | tf_op jit(solution)/shard_map/ppermute | solution.py:375
  198.7 9.3 %collective-permute-start.6 = (bf16[384,256]{1,0:T(8,128)(2,1)S(1)}, bf16[384,256]{1,0:T(8,128)(2,1)S(1)}, u32[]{:S(2)}, u32[]{:S(2)}) collective-permute-start(bf16[384,256]{1,0:T(8,128)(2,1)S(1)} %get-tuple-element.27), channel_id=1, source_target_pairs={{0,6},{2,0},{4,2},{6,4},{1,7},{3,1},{5,3},{7,5},{8,14},{10,8},{12,... | collective-permute-start | bytes 589832 | tf_op jit(solution)/shard_map/ppermute | solution.py:375
  201.5 8.7 %collective-permute-start.5 = (bf16[384,256]{1,0:T(8,128)(2,1)S(1)}, bf16[384,256]{1,0:T(8,128)(2,1)S(1)}, u32[]{:S(2)}, u32[]{:S(2)}) collective-permute-start(bf16[384,256]{1,0:T(8,128)(2,1)S(1)} %get-tuple-element.25), channel_id=1, source_target_pairs={{0,2},{2,4},{4,6},{6,0},{1,3},{3,5},{5,7},{7,1},{8,10},{10,12},{12... | collective-permute-start | bytes 589832 | tf_op jit(solution)/shard_map/ppermute | solution.py:375
Sparse Core Ops, SparseCore 0:
  11.2 170.8 all-gather.4

commit v8 on v5

--- a/solution.py
+++ b/solution.py
@@ -156,16 +156,21 @@
     bands, depth, _ = wide.shape
     gated = total.shape[1]
 
-    def band_copy(band):
+    def band_copy(band, down=False):
         row = pl.multiple_of(band * depth, depth)
+        columns = pl.ds(gated, weight.shape[1] - gated) if down else pl.ds(0, gated)
         return pltpu.make_async_copy(
-            weight.at[pl.ds(row, depth), :], wide.at[band], sems.at[band]
+            weight.at[pl.ds(row, depth), columns],
+            wide.at[band, :, columns],
+            sems.at[bands + band if down else band],
         )
 
-    feature_copy = pltpu.make_async_copy(features_at, features, sems.at[bands])
+    feature_copy = pltpu.make_async_copy(features_at, features, sems.at[2 * bands])
     feature_copy.start()
     for band in range(bands):
         band_copy(band).start()
+    for band in range(bands):
+        band_copy(band, True).start()
     factor = scale[...]
     feature_copy.wait()
     steps = [(at, min(2 * LANES, gated - at)) for at in range(0, gated, 2 * LANES)]
@@ -199,6 +204,7 @@
             value = jnp.where(lane < LANES // 2, activated(both, turned), 0.0)
         hidden[pair, :, side * LANES : (side + 1) * LANES] = value.astype(BF16)
     for chip in range(chips):
+        band_copy(chip, True).wait()
         theirs = pl.multiple_of((1 - core) * width, width)
         product = jnp.zeros((length, width), F32)
         for p in range(hidden.shape[0]):
@@ -352,7 +358,7 @@
             VM(features.shape, BF16),
             VM((chips, CORES * width, weight.shape[1]), BF16),
             VM((length, 2 * units), F32),
-            pltpu.SemaphoreType.DMA((chips + 1,)),
+            pltpu.SemaphoreType.DMA((2 * chips + 1,)),
         ),
         HIDDEN_VMEM,
     )(scal, features, scale_two, weight)

time: 217 us -> 219 us (level)
  no operation moved by 1% of the time
where the time goes in v8:
time: 219 us; the launch traced here: 218 us
  blocking collectives  117 us (53%)
  starting transfers between devices  56.7 us (26%)
  Pallas kernels  15.2 us (7%)
  between operations  13.6 us (6%)
  waiting for transfers between devices  12.1 us (6%)
    all_gather x1, blocking collectives, local(): mine = lax.all_gather(chosen, 'fs', axis=0, tiled=True)  53.8 us
    ppermute x3, starting transfers between devices, swap(): return lax.ppermute(array, 'core', [(0, 1), (1, 0)])  51.4 us
    all_gather x1, blocking collectives, local(): pooled_all = lax.all_gather(pooled, ('x', 'core'), axis=0)  24 us
    all_to_all x1, blocking collectives, local(): lax.all_to_all(paired, 'x', split_axis=0, concat_axis=0, tiled=True)  15.4 us
    all_gather x1, blocking collectives, local(): own = lax.all_gather(sent, 'x', axis=0)  12.2 us
    all_gather x1, blocking collectives, local(): own_two = lax.all_gather(scaled, 'x', axis=0)  12.2 us
    pallas_call x1, Pallas kernels, local(): call(hidden_kernel, (jax.ShapeDtypeStruct((blocks // 2, length, 2 * LANES...  8.08 us
    ppermute x1, waiting for transfers between devices, local(): theirs = lax.ppermute(mine, 'grp', [(i, i ^ 1) for i in range(groups)])  6.86 us
  transfers between devices with their start and end apart: 6, of which 4 were waited for; matrix products, arithmetic and copies ran while one was open for 0% of the time, Pallas kernels for 2%

profile of v8, /device:TPU:33, one launch (start us, length us, event | category | flops | bytes accessed | tf_op | source)
XLA Modules:
  0.0 218.2 jit_solution(13613668829934145370)
XLA Ops:
  6.6 2.1 shard_map.100
  8.7 1.6 collective-permute-start.3
  10.3 0.7 copy-done.5
  11.1 12.2 %all-gather = bf16[1600,256]{1,0:T(8,128)(2,1)S(1)} all-gather(bf16[400,256]{1,0:T(8,128)(2,1)} %get-tuple-element.14), channel_id=2, replica_groups=mesh['grp'=2,'fs'=32,'x'=4,'core'=2] {'x'}, dimensions={0}, use_global_device_ids=true | all-gather | bytes 1024000 | tf_op jit(solution)/shard_map/all_gather | solution.py:297
  23.3 44.8 %collective-permute-start = (bf16[4,400,256]{2,1,0:T(8,128)(2,1)S(1)}, bf16[4,400,256]{2,1,0:T(8,128)(2,1)S(1)}, u32[]{:S(2)}, u32[]{:S(2)}) collective-permute-start(bf16[4,400,256]{2,1,0:T(8,128)(2,1)S(1)} %bitcast.15), channel_id=1, source_target_pairs={{0,1},{1,0},{2,3},{3,2},{4,5},{5,4},{6,7},{7,6},{8,9},{9,8},{10,11... | collective-permute-start | bytes 2457608 | tf_op jit(solution)/shard_map/ppermute | solution.py:238
  68.1 53.8 %all_gather.26.mine = bf16[2048,128]{1,0:T(8,128)(2,1)S(1)} all-gather(bf16[64,128]{1,0:T(8,128)(2,1)S(1)} %maximum_select_fusion), channel_id=1, replica_groups=mesh['grp'=2,'fs'=32,'x'=4,'core'=2] {'fs'}, dimensions={0}, use_global_device_ids=true | all-gather | bytes 540672 | tf_op jit(solution)/shard_map/all_gather | solution.py:303
  121.9 3.7 %collective-permute-start.1 = (bf16[2048,128]{1,0:T(8,128)(2,1)S(1)}, bf16[2048,128]{1,0:T(8,128)(2,1)S(1)}, u32[]{:S(2)}, u32[]{:S(2)}) collective-permute-start(bf16[2048,128]{1,0:T(8,128)(2,1)S(1)} %all_gather.26.mine), channel_id=1, source_target_pairs={{0,256},{256,0},{1,257},{257,1},{2,258},{258,2},{3,259},{259,3},{4... | collective-permute-start | bytes 1572872 | tf_op jit(solution)/shard_map/ppermute | solution.py:305
  125.7 6.9 %collective-permute-done.1.theirs = bf16[2048,128]{1,0:T(8,128)(2,1)S(1)} collective-permute-done((bf16[2048,128]{1,0:T(8,128)(2,1)S(1)}, bf16[2048,128]{1,0:T(8,128)(2,1)S(1)}, u32[]{:S(2)}, u32[]{:S(2)}) %collective-permute-start.1) | collective-permute-done | bytes 524320 | tf_op jit(solution)/shard_map/ppermute | solution.py:305
  132.6 2.0 shard_map.101
  134.6 24.0 %all-gather.1 = bf16[3072,128]{1,0:T(8,128)(2,1)S(1)} all-gather(bf16[384,128]{1,0:T(8,128)(2,1)S(1)} %shard_map.101), channel_id=3, replica_groups=mesh['grp'=2,'fs'=32,'x'=4,'core'=2] {'x','core'}, dimensions={0}, use_global_device_ids=true | all-gather | bytes 884736 | tf_op jit(solution)/shard_map/all_gather | solution.py:314
  158.7 1.2 shard_map.102
  159.8 12.2 %all-gather.2 = bf16[1536,256]{1,0:T(8,128)(2,1)S(1)} all-gather(bf16[384,256]{1,0:T(8,128)(2,1)S(1)} %get-tuple-element.16), channel_id=4, replica_groups=mesh['grp'=2,'fs'=32,'x'=4,'core'=2] {'x'}, dimensions={0}, use_global_device_ids=true | all-gather | bytes 983040 | tf_op jit(solution)/shard_map/all_gather | solution.py:334
  172.0 3.7 %collective-permute-start.2 = (bf16[4,384,256]{2,1,0:T(8,128)(2,1)S(1)}, bf16[4,384,256]{2,1,0:T(8,128)(2,1)S(1)}, u32[]{:S(2)}, u32[]{:S(2)}) collective-permute-start(bf16[4,384,256]{2,1,0:T(8,128)(2,1)S(1)} %bitcast.20), channel_id=1, source_target_pairs={{0,1},{1,0},{2,3},{3,2},{4,5},{5,4},{6,7},{7,6},{8,9},{9,8},{10,11... | collective-permute-start | bytes 2359304 | tf_op jit(solution)/shard_map/ppermute | solution.py:238
  175.7 1.9 collective-permute-done.2.other
  177.6 1.1 shard_map.103
  178.7 1.1 copy-done
  179.9 2.2 %all-gather.5.cloned.1.call-done.weight = bf16[2048,2176]{1,0:T(8,128)(2,1)} async-done(((bf16[64,2176]{1,0:T(8,128)(2,1)}), bf16[2048,2176]{1,0:T(8,128)(2,1)}) %all-gather.5.cloned.1.call-update) | async-done | bytes 8912912 | tf_op jit(solution)/shard_map/all_gather | solution.py:293
  182.0 8.1 %shard_map.104 = (bf16[3,384,256]{2,1,0:T(8,128)(2,1)S(1)}, bf16[4,384,256]{2,1,0:T(8,128)(2,1)S(1)}, bf16[4,256,768]{2,1,0:T(8,128)(2,1)S(1)}) custom-call(s32[3]{0:T(128)S(1)} %pad_add_fusion.scal, bf16[4,384,512]{2,1,0:T(8,128)(2,1)} %copy-done, f32[384,128]{1,0:T(8,128)S(1)} %get-tuple-element.18.scale, ...), custom_call_target="tpu_custom_call" | custom-call | flops 2768240640 | bytes 8650752 | tf_op jit(solution)/shard_map/pallas_call | solution.py:347
  190.1 2.8 %collective-permute-start.4 = (bf16[4,384,256]{2,1,0:T(8,128)(2,1)S(1)}, bf16[4,384,256]{2,1,0:T(8,128)(2,1)S(1)}, u32[]{:S(2)}, u32[]{:S(2)}) collective-permute-start(bf16[4,384,256]{2,1,0:T(8,128)(2,1)S(1)} %get-tuple-element.22), channel_id=1, source_target_pairs={{0,1},{1,0},{2,3},{3,2},{4,5},{5,4},{6,7},{7,6},{8,9},{9,8},{10,11... | collective-permute-start | bytes 2359304 | tf_op jit(solution)/shard_map/ppermute | solution.py:238
  193.0 0.8 shard_map.105
  193.8 1.1 collective-permute-done.4
  194.9 0.3 add_convert_fusion
  195.1 15.4 %all_to_all.5 = bf16[4,384,256]{2,1,0:T(8,128)(2,1)S(1)} all-to-all(bf16[4,384,256]{2,1,0:T(8,128)(2,1)S(1)} %add_convert_fusion), channel_id=1, replica_groups=mesh['grp'=2,'fs'=32,'x'=4,'core'=2] {'x'}, dimensions={0} | all-to-all | bytes 1572864 | tf_op jit(solution)/shard_map/all_to_all | solution.py:374
  210.6 0.7 fusion
  (22 shorter events, 0.3 us)
Async XLA Ops:
  6.5 61.6 %copy-start.7 = (bf16[32,256]{1,0:T(8,128)(2,1)S(1)}, bf16[32,256]{1,0:T(8,128)(2,1)}, u32[]{:S(2)}) copy-start(bf16[32,256]{1,0:T(8,128)(2,1)} %param.15) | copy-start | bytes 49156
  6.5 61.6 %copy-start.6 = (bf16[64,128]{1,0:T(8,128)(2,1)S(1)}, bf16[64,128]{1,0:T(8,128)(2,1)}, u32[]{:S(2)}) copy-start(bf16[64,128]{1,0:T(8,128)(2,1)} %param.12) | copy-start | bytes 49156
  6.6 126.0 %copy-start.2 = (bf16[1,128,128]{2,1,0:T(8,128)(2,1)S(1)}, bf16[1,128,128]{2,1,0:T(8,128)(2,1)}, u32[]{:S(2)}) copy-start(bf16[1,128,128]{2,1,0:T(8,128)(2,1)} %pool_weight.1) | copy-start | bytes 98308
  6.6 126.0 %copy-start.4 = (f32[128]{0:T(128)S(1)}, f32[128]{0:T(128)}, u32[]{:S(2)}) copy-start(f32[128]{0:T(128)} %param.14) | copy-start | bytes 1540
  6.6 175.5 %all-gather.5.cloned.1.call-start = ((), (), s32[]{:S(2)}) async-start(), calls=%async_computation.1 | async-start | bytes 9191424 | tf_op jit(solution)/shard_map/all_gather | solution.py:293
  8.7 1.6 collective-permute-start.3
  10.3 0.7 copy-start.5
  23.3 109.3 %collective-permute-start = (bf16[4,400,256]{2,1,0:T(8,128)(2,1)S(1)}, bf16[4,400,256]{2,1,0:T(8,128)(2,1)S(1)}, u32[]{:S(2)}, u32[]{:S(2)}) collective-permute-start(bf16[4,400,256]{2,1,0:T(8,128)(2,1)S(1)} %bitcast.15), channel_id=1, source_target_pairs={{0,1},{1,0},{2,3},{3,2},{4,5},{5,4},{6,7},{7,6},{8,9},{9,8},{10,11... | collective-permute-start | bytes 2457608 | tf_op jit(solution)/shard_map/ppermute | solution.py:238
  121.9 10.7 %collective-permute-start.1 = (bf16[2048,128]{1,0:T(8,128)(2,1)S(1)}, bf16[2048,128]{1,0:T(8,128)(2,1)S(1)}, u32[]{:S(2)}, u32[]{:S(2)}) collective-permute-start(bf16[2048,128]{1,0:T(8,128)(2,1)S(1)} %all_gather.26.mine), channel_id=1, source_target_pairs={{0,256},{256,0},{1,257},{257,1},{2,258},{258,2},{3,259},{259,3},{4... | collective-permute-start | bytes 1572872 | tf_op jit(solution)/shard_map/ppermute | solution.py:305
  132.6 26.1 %copy-start.1 = (bf16[1,384,256]{2,1,0:T(8,128)(2,1)S(1)}, bf16[1,384,256]{2,1,0:T(8,128)(2,1)}, u32[]{:S(2)}) copy-start(bf16[1,384,256]{2,1,0:T(8,128)(2,1)} %param.10) | copy-start | bytes 589828
  132.6 26.1 %copy-start.3 = (f32[256]{0:T(256)S(1)}, f32[256]{0:T(256)}, u32[]{:S(2)}) copy-start(f32[256]{0:T(256)} %param.16) | copy-start | bytes 3076
  172.0 5.6 %collective-permute-start.2 = (bf16[4,384,256]{2,1,0:T(8,128)(2,1)S(1)}, bf16[4,384,256]{2,1,0:T(8,128)(2,1)S(1)}, u32[]{:S(2)}, u32[]{:S(2)}) collective-permute-start(bf16[4,384,256]{2,1,0:T(8,128)(2,1)S(1)} %bitcast.20), channel_id=1, source_target_pairs={{0,1},{1,0},{2,3},{3,2},{4,5},{5,4},{6,7},{7,6},{8,9},{9,8},{10,11... | collective-permute-start | bytes 2359304 | tf_op jit(solution)/shard_map/ppermute | solution.py:238
  178.7 1.1 copy-start
  190.1 4.7 %collective-permute-start.4 = (bf16[4,384,256]{2,1,0:T(8,128)(2,1)S(1)}, bf16[4,384,256]{2,1,0:T(8,128)(2,1)S(1)}, u32[]{:S(2)}, u32[]{:S(2)}) collective-permute-start(bf16[4,384,256]{2,1,0:T(8,128)(2,1)S(1)} %get-tuple-element.22), channel_id=1, source_target_pairs={{0,1},{1,0},{2,3},{3,2},{4,5},{5,4},{6,7},{7,6},{8,9},{9,8},{10,11... | collective-permute-start | bytes 2359304 | tf_op jit(solution)/shard_map/ppermute | solution.py:238
Sparse Core Ops, SparseCore 0:
  11.2 170.7 all-gather.4
